TPU v7x, 32 devices: a whole 2x2x4 slice. The times are simulated.
32 devices in a mesh: sp: 8 (over z, y), dp: 4 (over x, core).
Axes of the slice: x: 2, y: 2, z: 4, core: 2. Of those that a mesh axis runs over, the one named last changes fastest.
Arguments:
- queries: bfloat16 [4, 1024, 16, 128], P('dp', 'sp'), may hold values from -7 to 7
- key_vectors: bfloat16 [4, 1024, 16, 128], P('dp', 'sp'), may hold values from -6 to 6
- value_vectors: bfloat16 [4, 1024, 16, 128], P('dp', 'sp'), may hold values from -6 to 6
- head_lambda: float32 [16], P('sp'), may hold values from 0.3 to 0.8
- head_gain: float32 [128], replicated, may hold values from 0.1 to 1.9
- residual: bfloat16 [4, 1024, 2048], P('dp', 'sp'), may hold values from -6 to 6
- out_weight: bfloat16 [2048, 2048], replicated, may hold values from -0.125 to 0.125
- mix_gain: float32 [2048], replicated, may hold values from 0.1 to 1.9
- pre_gain: float32 [2048], replicated, may hold values from 0.1 to 1.9
- post_gain: float32 [2048], replicated, may hold values from 0.1 to 1.9
- routes: int32 [4, 1024, 4], P('dp', 'sp'), may hold values from 0 to 31, all different within a row; in each aligned block of 128 rows (0 to 127, 128 to 255, ..., all dimensions but the last counted through in order) at most 24 rows name the same one
- route_weights: float32 [4, 1024, 4], P('dp', 'sp'), may hold values from 0.25 to 1
- expert_gate: bfloat16 [32, 2048, 512], P(('sp', 'dp')), may hold values from -0.125 to 0.125
- expert_up: bfloat16 [32, 2048, 512], P(('sp', 'dp')), may hold values from -0.125 to 0.125
- expert_down: bfloat16 [32, 512, 2048], P(('sp', 'dp')), may hold values from -0.25 to 0.25
- shared_gate: bfloat16 [2048, 512], replicated, may hold values from -0.125 to 0.125
- shared_up: bfloat16 [2048, 512], replicated, may hold values from -0.125 to 0.125
- shared_down: bfloat16 [512, 2048], replicated, may hold values from -0.25 to 0.25
Outputs:
- output: bfloat16 [4, 1024, 2048], P('dp', 'sp')
Inputs may be any that keep to these rules, and one draw needn't show every extreme that they name: `routes`: among the tokens of one device (aligned blocks of 128 positions), no expert is named more than 24 times; in some block some expert is named exactly 24 times. Each token names 4 different experts.
All inputs are finite; a program needn't handle non-finite values.
Results may differ from a plain program's by a relative error of at most 0.0075.
Values may be sent and summed in bfloat16 or wider, within the bound.
A program may use at most 128 MiB of HBM per device.

v0:
```python
import jax
import jax.numpy as jnp
from jax import lax
from jax.sharding import PartitionSpec as P

epsilon = 1e-06


def rms_scale(values_in, gain):
    return (
        values_in
        * lax.rsqrt(jnp.mean(values_in * values_in, axis=-1, keepdims=True) + epsilon)
        * gain
    )


def feed_forward(rows, gate_w, up_w, down_w):
    gate_val = jnp.dot(rows, gate_w, preferred_element_type=jnp.float32)
    up_val = jnp.dot(rows, up_w, preferred_element_type=jnp.float32)
    hidden = (jax.nn.silu(gate_val) * up_val).astype(jnp.bfloat16)
    return jnp.dot(hidden, down_w, preferred_element_type=jnp.float32).astype(jnp.bfloat16)


def attend_heads(query_heads, key_heads, value_heads, head_lambda, head_gain):
    length = query_heads.shape[0]
    head_count = query_heads.shape[1]
    head_size = query_heads.shape[2] // 2
    block_rows = min(512, length)
    block_count = length // block_rows
    query_blocks = query_heads.reshape(block_count, block_rows, head_count, 2, head_size)
    key_all = key_heads.reshape(length, head_count, 2, head_size)
    key_pos = jnp.arange(length, dtype=jnp.int32)

    def one_block(inputs):
        query_block, block_index = inputs
        scores = jnp.einsum(
            "qhmd,khmd->hmqk", query_block, key_all, preferred_element_type=jnp.float32
        ) * head_size ** (-0.5)
        query_pos = block_index * block_rows + jnp.arange(block_rows, dtype=jnp.int32)
        causal = key_pos[None, :] <= query_pos[:, None]
        scores = jnp.where(causal, scores, -jnp.inf)
        maxima = jnp.max(scores, axis=-1, keepdims=True)
        exponent = jnp.exp(scores - maxima)
        softmax_both = exponent / jnp.sum(exponent, axis=-1, keepdims=True)
        mixture = (softmax_both[:, 0] - head_lambda[:, None, None] * softmax_both[:, 1]).astype(
            jnp.bfloat16
        )
        head_output = jnp.einsum(
            "hqk,khe->qhe", mixture, value_heads, preferred_element_type=jnp.float32
        )
        return rms_scale(head_output, head_gain).astype(jnp.bfloat16)

    outputs = lax.map(one_block, (query_blocks, jnp.arange(block_count, dtype=jnp.int32)))
    return outputs.reshape(length, head_count, -1)


def local(
    queries,
    key_vectors,
    value_vectors,
    head_lambda,
    head_gain,
    residual,
    out_weight,
    mix_gain,
    pre_gain,
    post_gain,
    routes,
    route_weights,
    expert_gate,
    expert_up,
    expert_down,
    shared_gate,
    shared_up,
    shared_down,
):
    query_heads, key_heads, value_heads = (
        lax.all_to_all(queries[0], "sp", split_axis=1, concat_axis=0, tiled=True),
        lax.all_to_all(key_vectors[0], "sp", split_axis=1, concat_axis=0, tiled=True),
        lax.all_to_all(value_vectors[0], "sp", split_axis=1, concat_axis=0, tiled=True),
    )
    attended = attend_heads(query_heads, key_heads, value_heads, head_lambda, head_gain)
    token_heads = lax.all_to_all(attended, "sp", split_axis=0, concat_axis=1, tiled=True)
    tok_count = token_heads.shape[0]
    flat_heads = token_heads.reshape(tok_count, -1)
    mixed_rows = jnp.dot(flat_heads, out_weight, preferred_element_type=jnp.float32)
    updated = (residual[0].astype(jnp.float32) + rms_scale(mixed_rows, mix_gain)).astype(
        jnp.bfloat16
    )
    normed = rms_scale(updated.astype(jnp.float32), pre_gain).astype(jnp.bfloat16)
    model_width = normed.shape[1]
    experts_total = lax.axis_size("sp") * lax.axis_size("dp")
    top_count = routes.shape[2]
    capacity = 3 * tok_count * top_count // (2 * experts_total)
    assign_count = tok_count * top_count
    flat_routes = routes[0].reshape(assign_count)
    one_hot = (flat_routes[:, None] == jnp.arange(experts_total, dtype=jnp.int32)[None, :]).astype(
        jnp.int32
    )
    earlier = jnp.cumsum(one_hot, axis=0) - one_hot
    rank_index = jnp.sum(earlier * one_hot, axis=1)
    slot_index = flat_routes * capacity + rank_index
    source_row = (
        jnp.zeros((experts_total * capacity,), jnp.int32)
        .at[slot_index]
        .set(jnp.arange(assign_count, dtype=jnp.int32) // top_count)
    )
    occupied = (
        jnp.zeros((experts_total * capacity,), jnp.bfloat16)
        .at[slot_index]
        .set(jnp.ones((assign_count,), jnp.bfloat16))
    )
    outgoing = (normed[source_row] * occupied[:, None]).reshape(
        experts_total, capacity, model_width
    )
    shared_out = feed_forward(normed, shared_gate, shared_up, shared_down)
    arrived = lax.all_to_all(outgoing, ("sp", "dp"), split_axis=0, concat_axis=0, tiled=True)
    flat_rows = arrived.reshape(-1, model_width)
    result_rows = feed_forward(flat_rows, expert_gate[0], expert_up[0], expert_down[0])
    results = result_rows.reshape(arrived.shape[0], -1, model_width)
    returned = lax.all_to_all(results, ("sp", "dp"), split_axis=0, concat_axis=0, tiled=True)
    picked = returned.reshape(experts_total * capacity, model_width)[slot_index]
    routed = jnp.sum(
        picked.astype(jnp.float32).reshape(tok_count, top_count, model_width)
        * route_weights[0][:, :, None],
        axis=1,
    )
    combined = routed + shared_out.astype(jnp.float32)
    output = (updated.astype(jnp.float32) + rms_scale(combined, post_gain)).astype(jnp.bfloat16)
    return output.reshape(1, tok_count, model_width)


def solution(mesh):
    in_specs = (
        P("dp", "sp", None, None),
        P("dp", "sp", None, None),
        P("dp", "sp", None, None),
        P("sp"),
        P(),
        P("dp", "sp", None),
        P(),
        P(),
        P(),
        P(),
        P("dp", "sp", None),
        P("dp", "sp", None),
        P(("sp", "dp"), None, None),
        P(("sp", "dp"), None, None),
        P(("sp", "dp"), None, None),
        P(),
        P(),
        P(),
    )
    out_specs = P("dp", "sp", None)
    return jax.shard_map(local, mesh=mesh, in_specs=in_specs, out_specs=out_specs, check_vma=False)
```

profile of v0, /device:TPU:0, one launch (start us, length us, event | category | flops | bytes accessed | tf_op | source)
XLA Modules:
  0.0 313.4 jit_solution(17790925592510892741)
XLA Ops:
  0.0 2.1 copy.77
  2.1 7.3 %all-to-all-start = ((bf16[128,16,128]{2,0,1:T(8,128)(2,1)}), bf16[128,16,128]{2,0,1:T(8,128)(2,1)S(1)}, u32[]{:S(2)}, u32[]{:S(2)}) async-start(bf16[128,16,128]{2,0,1:T(8,128)(2,1)} %bitcast.132), calls=%async_computation | async-start | bytes 1048576 | tf_op jit(solution)/shard_map/all_to_all | solution.py:78
  9.4 2.0 copy.75
  11.4 12.5 %all-to-all-done = bf16[128,16,128]{2,0,1:T(8,128)(2,1)S(1)} async-done(((bf16[128,16,128]{2,0,1:T(8,128)(2,1)}), bf16[128,16,128]{2,0,1:T(8,128)(2,1)S(1)}, u32[]{:S(2)}, u32[]{:S(2)}) %all-to-all-start) | async-done | bytes 524320 | tf_op jit(solution)/shard_map/all_to_all | solution.py:78
  23.9 3.6 %all-to-all-start.2 = ((bf16[128,16,128]{2,0,1:T(8,128)(2,1)}), bf16[128,16,128]{2,0,1:T(8,128)(2,1)S(1)}, u32[]{:S(2)}, u32[]{:S(2)}) async-start(bf16[128,16,128]{2,0,1:T(8,128)(2,1)} %bitcast.155), calls=%async_computation.2 | async-start | bytes 1048576 | tf_op jit(solution)/shard_map/all_to_all | solution.py:80
  27.6 2.0 copy.76
  29.5 12.7 %all-to-all-done.2 = bf16[128,16,128]{2,0,1:T(8,128)(2,1)S(1)} async-done(((bf16[128,16,128]{2,0,1:T(8,128)(2,1)}), bf16[128,16,128]{2,0,1:T(8,128)(2,1)S(1)}, u32[]{:S(2)}, u32[]{:S(2)}) %all-to-all-start.2) | async-done | bytes 524320 | tf_op jit(solution)/shard_map/all_to_all | solution.py:80
  42.2 4.1 %all-to-all-start.1 = ((bf16[128,16,128]{2,0,1:T(8,128)(2,1)}), bf16[128,16,128]{2,0,1:T(8,128)(2,1)}, u32[]{:S(2)}, u32[]{:S(2)}) async-start(bf16[128,16,128]{2,0,1:T(8,128)(2,1)} %bitcast.154), calls=%async_computation.1 | async-start | bytes 1048576 | tf_op jit(solution)/shard_map/all_to_all | solution.py:79
  46.4 0.1 copy.63
  46.5 0.1 eq.29
  46.6 0.1 eq.25
  46.8 1.2 reduce-window.6
  47.9 0.2 slice_reduce_fusion
  48.2 1.1 copy.52
  49.3 1.3 reshape.133
  50.6 0.9 copy.57
  51.5 0.3 copy.56
  51.8 1.1 all_to_all.61
  52.8 7.8 %all-to-all-done.1 = bf16[128,16,128]{2,0,1:T(8,128)(2,1)} async-done(((bf16[128,16,128]{2,0,1:T(8,128)(2,1)}), bf16[128,16,128]{2,0,1:T(8,128)(2,1)}, u32[]{:S(2)}, u32[]{:S(2)}) %all-to-all-start.1) | async-done | bytes 524320 | tf_op jit(solution)/shard_map/all_to_all | solution.py:79
  60.7 1.3 copy.54
  62.0 1.1 reshape.134
  63.1 29.6 %while.11 = (s32[]{:T(128)}, bf16[2,512,2,128]{3,1,0,2:T(8,128)(2,1)}, s32[2]{0:T(128)S(1)}, bf16[2,512,2,2,64]{1,4,3,2,0:T(8,128)(2,1)S(1)}, bf16[1024,2,2,64]{...) while((s32[]{:T(128)}, ...), condition=%wide.region_4.5_spmd.clone, body=%wide.region_0.4_spmd.clone.sunk | while | flops 551684608 | bytes 40408232 | solution.py:53
  63.1 0.7 dynamic_slice.29
  64.5 0.4 iota_compare_fusion.4
  64.9 7.1 %fusion.99 = (f32[2,2,512]{2,1,0:T(2,128)S(1)}, f32[2,2,512,1024]{3,2,1,0:T(8,128)}) fusion(pred[512,1024]{1,0:T(8,128)(4,1)S(1)} %iota_compare_fusion.4, bf16[1024,2,2,64]{0,3,2,1:T(8,128)(2,1)} %get-tuple-element.202, bf16[2,512,2,2,64]{1,4,3,2,0:T(8,128)(2,1)S(1)} %get-tuple-element.201, s32[]{:T(128)} %get-tuple-element.188), kind=kOutput, calls=%fused_computation.102.clone.1 | convolution fusion | flops 276825088 | bytes 9707524 | tf_op jit(solution)/shard_map/while/body/eval_jaxpr/sub | solution.py:43
  72.0 4.0 %broadcast_divide_fusion.2 = f32[2,2,512,1024]{3,2,1,0:T(8,128)S(1)} fusion(f32[2,2,512,1024]{3,2,1,0:T(8,128)} %get-tuple-element.174, f32[2,2,512]{2,1,0:T(2,128)S(1)} %get-tuple-element.175), kind=kLoop, calls=%fused_computation.14.clone.1 | loop fusion | flops 2097152 | bytes 16785408 | tf_op jit(solution)/shard_map/while/body/eval_jaxpr/div | solution.py:44
  76.0 0.9 multiply_reduce_fusion.5
  76.9 0.1 fusion.100
  77.0 0.2 copy.79
  77.2 0.7 constant_dynamic-update-slice_fusion.2
  77.9 0.7 dynamic_slice.29
  79.3 0.4 iota_compare_fusion.4
  79.7 7.1 %fusion.99 = (f32[2,2,512]{2,1,0:T(2,128)S(1)}, f32[2,2,512,1024]{3,2,1,0:T(8,128)}) fusion(pred[512,1024]{1,0:T(8,128)(4,1)S(1)} %iota_compare_fusion.4, bf16[1024,2,2,64]{0,3,2,1:T(8,128)(2,1)} %get-tuple-element.202, bf16[2,512,2,2,64]{1,4,3,2,0:T(8,128)(2,1)S(1)} %get-tuple-element.201, s32[]{:T(128)} %get-tuple-element.188), kind=kOutput, calls=%fused_computation.102.clone.1 | convolution fusion | flops 276825088 | bytes 9707524 | tf_op jit(solution)/shard_map/while/body/eval_jaxpr/sub | solution.py:43
  86.8 4.0 %broadcast_divide_fusion.2 = f32[2,2,512,1024]{3,2,1,0:T(8,128)S(1)} fusion(f32[2,2,512,1024]{3,2,1,0:T(8,128)} %get-tuple-element.174, f32[2,2,512]{2,1,0:T(2,128)S(1)} %get-tuple-element.175), kind=kLoop, calls=%fused_computation.14.clone.1 | loop fusion | flops 2097152 | bytes 16785408 | tf_op jit(solution)/shard_map/while/body/eval_jaxpr/div | solution.py:44
  90.8 0.9 multiply_reduce_fusion.5
  91.7 0.1 fusion.100
  91.8 0.2 copy.79
  92.0 0.7 constant_dynamic-update-slice_fusion.2
  92.7 2.4 copy.59
  95.1 3.6 %all-to-all-start.3 = ((bf16[1024,2,128]{2,1,0:T(2,128)(2,1)}), bf16[1024,2,128]{2,1,0:T(2,128)(2,1)S(1)}, u32[]{:S(2)}, u32[]{:S(2)}) async-start(bf16[1024,2,128]{2,1,0:T(2,128)(2,1)} %copy.59), calls=%async_computation.3 | async-start | bytes 1048576 | tf_op jit(solution)/shard_map/all_to_all | solution.py:83
  98.7 0.1 copy.62
  98.9 0.1 mul.159
  99.1 2.6 scatter_custom_fusion
  101.7 3.8 %scatter_custom_fusion.1 = bf16[768]{0:T(1024)(128)(2,1)S(1)} fusion(s32[512]{0:T(512)S(1)} %bitcast.160, bf16[512]{0:T(512)(128)(2,1)S(1)} %broadcast.140, bf16[]{:T(256)} %constant.60.clone.1), kind=kCustom, calls=%fused_computation.94 | custom fusion | bytes 1538 | tf_op jit(solution)/shard_map/scatter | solution.py:111
  105.6 7.6 %all-to-all-done.3 = bf16[1024,2,128]{2,1,0:T(2,128)(2,1)S(1)} async-done(((bf16[1024,2,128]{2,1,0:T(2,128)(2,1)}), bf16[1024,2,128]{2,1,0:T(2,128)(2,1)S(1)}, u32[]{:S(2)}, u32[]{:S(2)}) %all-to-all-start.3) | async-done | bytes 524320 | tf_op jit(solution)/shard_map/all_to_all | solution.py:83
  113.4 0.3 copy.61
  113.7 4.8 %multiply_reduce_fusion.3 = (f32[128]{0:T(128)S(1)}, f32[128,2048]{1,0:T(8,128)S(1)}) fusion(bf16[128,2048]{0,1:T(8,128)(2,1)S(1)} %bitcast.148, bf16[2048,2048]{1,0:T(8,128)(2,1)} %param.26), kind=kOutput, calls=%fused_computation.61 | convolution fusion | flops 1074265984 | bytes 9961984 | tf_op jit(solution)/shard_map/dot_general | solution.py:86
  118.5 0.4 fusion.45
  118.9 0.2 fusion.47
  119.1 4.3 %gather_fusion = bf16[768,2048]{1,0:T(8,128)(2,1)} fusion(bf16[128,2048]{1,0:T(8,128)(2,1)S(1)} %fusion.47, s32[1024]{0:T(1024)S(1)} %pad_clamp_fusion.1), kind=kCustom, calls=%fused_computation | custom fusion | bytes 6294528 | tf_op jit(solution)/shard_map/gather | solution.py:113
  123.4 2.2 broadcast_multiply_fusion
  125.5 74.6 %all_to_all.73 = bf16[32,24,2048]{2,1,0:T(8,128)(2,1)S(1)} all-to-all(bf16[32,24,2048]{2,1,0:T(8,128)(2,1)S(1)} %broadcast_multiply_fusion), channel_id=1, replica_groups=mesh['sp'=8,'dp'=4] {'sp','dp'}, dimensions={0} | all-to-all | bytes 6291456 | tf_op jit(solution)/shard_map/all_to_all | solution.py:117
  200.1 1.7 copy-done.1
  201.8 2.9 fusion.40
  204.8 8.1 %convolution_convert_fusion = bf16[768,2048]{1,0:T(8,128)(2,1)} fusion(bf16[1,512,2048]{2,1,0:T(8,128)(2,1)S(1)} %copy-done, f32[768,512]{1,0:T(8,128)} %fusion.40, bf16[768,2048]{1,0:T(8,128)(2,1)} %bitcast.151, bf16[1,2048,512]{2,1,0:T(8,128)(2,1)} %param.33), kind=kOutput, calls=%fused_computation.38 | convolution fusion | flops 3225157632 | bytes 12058624 | tf_op jit(solution)/shard_map/dot_general | solution.py:21
  212.9 4.0 %all-to-all-start.5 = ((bf16[32,24,2048]{2,1,0:T(8,128)(2,1)}), bf16[32,24,2048]{2,1,0:T(8,128)(2,1)}, u32[]{:S(2)}, u32[]{:S(2)}) async-start(bf16[32,24,2048]{2,1,0:T(8,128)(2,1)} %bitcast.149), calls=%async_computation.5 | async-start | bytes 6291456 | tf_op jit(solution)/shard_map/all_to_all | solution.py:121
  216.9 0.1 copy.66
  217.1 2.0 fusion.78
  219.1 69.1 %all-to-all-done.5 = bf16[32,24,2048]{2,1,0:T(8,128)(2,1)} async-done(((bf16[32,24,2048]{2,1,0:T(8,128)(2,1)}), bf16[32,24,2048]{2,1,0:T(8,128)(2,1)}, u32[]{:S(2)}, u32[]{:S(2)}) %all-to-all-start.5) | async-done | bytes 3145760 | tf_op jit(solution)/shard_map/all_to_all | solution.py:121
  288.2 7.5 %gather_fusion.1 = bf16[512,2048]{1,0:T(8,128)(2,1)} fusion(bf16[768,2048]{1,0:T(8,128)(2,1)} %bitcast.23, s32[1024]{0:T(1024)S(1)} %pad_clamp_fusion), kind=kCustom, calls=%fused_computation.1 | custom fusion | bytes 4196352 | tf_op jit(solution)/shard_map/gather | solution.py:122
  295.7 4.8 %reshape.143 = f32[128,4,2048]{2,1,0:T(4,128)} reshape(bf16[512,2048]{1,0:T(8,128)(2,1)} %gather_fusion.1) | data formatting | bytes 6291456 | tf_op jit(solution)/shard_map/convert_element_type | solution.py:124
  300.4 6.3 %multiply_reduce_fusion.1 = f32[128,2048]{1,0:T(8,128)} fusion(f32[128,4,2048]{2,1,0:T(4,128)} %reshape.143, f32[128,4]{1,0:T(8,128)S(1)} %copy.66), kind=kLoop, calls=%fused_computation.37 | loop fusion | flops 1835008 | bytes 5244928 | tf_op jit(solution)/shard_map/reduce_sum | solution.py:123
  306.8 4.3 %multiply_reduce_fusion.2 = (f32[128]{0:T(128)S(1)}, f32[128,2048]{1,0:T(8,128)}) fusion(f32[128,2048]{1,0:T(8,128)} %multiply_reduce_fusion.1, bf16[512,2048]{1,0:T(8,128)(2,1)} %param.37, bf16[128,2048]{1,0:T(8,128)(2,1)S(1)} %fusion.47, bf16[2048,512]{1,0:T(8,128)(2,1)} %param.36, f32[128,512]{1,0:T(8,128)S(1)} %fusion.78), kind=kOutput, calls=%fused_computation.60 | convolution fusion | flops 538574720 | bytes 7078400 | tf_op jit(solution)/shard_map/dot_general | solution.py:21
  311.1 2.2 fusion.52
  (52 shorter events, 0.5 us)
Async XLA Ops:
  0.0 204.8 %copy-start = (bf16[1,512,2048]{2,1,0:T(8,128)(2,1)S(1)}, bf16[1,512,2048]{2,1,0:T(8,128)(2,1)}, u32[]{:S(2)}) copy-start(bf16[1,512,2048]{2,1,0:T(8,128)(2,1)} %param.34) | copy-start | bytes 6291460
  0.0 46.4 %copy-start.10 = (s32[1,128,4]{1,2,0:T(4,128)S(1)}, s32[1,128,4]{1,2,0:T(4,128)}, u32[]{:S(2)}) copy-start(s32[1,128,4]{1,2,0:T(4,128)} %param.30) | copy-start | bytes 6148
  2.1 21.8 %all-to-all-start = ((bf16[128,16,128]{2,0,1:T(8,128)(2,1)}), bf16[128,16,128]{2,0,1:T(8,128)(2,1)S(1)}, u32[]{:S(2)}, u32[]{:S(2)}) async-start(bf16[128,16,128]{2,0,1:T(8,128)(2,1)} %bitcast.132), calls=%async_computation | async-start | bytes 1048576 | tf_op jit(solution)/shard_map/all_to_all | solution.py:78
  23.9 18.3 %all-to-all-start.2 = ((bf16[128,16,128]{2,0,1:T(8,128)(2,1)}), bf16[128,16,128]{2,0,1:T(8,128)(2,1)S(1)}, u32[]{:S(2)}, u32[]{:S(2)}) async-start(bf16[128,16,128]{2,0,1:T(8,128)(2,1)} %bitcast.155), calls=%async_computation.2 | async-start | bytes 1048576 | tf_op jit(solution)/shard_map/all_to_all | solution.py:80
  42.2 18.4 %all-to-all-start.1 = ((bf16[128,16,128]{2,0,1:T(8,128)(2,1)}), bf16[128,16,128]{2,0,1:T(8,128)(2,1)}, u32[]{:S(2)}, u32[]{:S(2)}) async-start(bf16[128,16,128]{2,0,1:T(8,128)(2,1)} %bitcast.154), calls=%async_computation.1 | async-start | bytes 1048576 | tf_op jit(solution)/shard_map/all_to_all | solution.py:79
  48.2 13.8 %copy-start.6 = (s32[32,5]{0,1:T(8,128)}, s32[32,5]{0,1:T(8,128)S(1)}, u32[]{:S(2)}) copy-start(s32[32,5]{0,1:T(8,128)S(1)} %reduce-window.9) | copy-start | bytes 1924
  49.3 13.8 %copy-start.5 = (f32[128]{0:T(128)S(1)}, f32[128]{0:T(128)}, u32[]{:S(2)}) copy-start(f32[128]{0:T(128)} %param.24) | copy-start | bytes 1540
  49.3 13.8 %copy-start.13 = (f32[2]{0:T(128)S(1)}, f32[2]{0:T(128)}, u32[]{:S(2)}) copy-start(f32[2]{0:T(128)} %param.23) | copy-start | bytes 28
  51.8 11.3 %copy-start.2 = (bf16[2,512,2,2,64]{1,4,3,2,0:T(8,128)(2,1)S(1)}, bf16[2,512,2,2,64]{1,4,3,2,0:T(8,128)(2,1)}, u32[]{:S(2)}) copy-start(bf16[2,512,2,2,64]{1,4,3,2,0:T(8,128)(2,1)} %copy.57) | copy-start | bytes 1572868
  63.1 35.9 %slice-start = ((s32[32,5]{0,1:T(8,128)}), s32[32,4]{0,1:T(4,128)S(1)}, s32[]{:S(2)}) async-start(s32[32,5]{0,1:T(8,128)} %copy-done.6), calls=%async_computation.6 | async-start | bytes 4096 | tf_op jit(solution)/shard_map/slice.1
  72.0 4.0 %copy-start.3 = (bf16[1024,2,128]{0,2,1:T(8,128)(2,1)S(1)}, bf16[1024,2,128]{0,2,1:T(8,128)(2,1)}, u32[]{:S(2)}) copy-start(bf16[1024,2,128]{0,2,1:T(8,128)(2,1)} %get-tuple-element.204) | copy-start | bytes 1572868 | tf_op jit(solution)/shard_map/while
  86.8 4.0 %copy-start.3 = (bf16[1024,2,128]{0,2,1:T(8,128)(2,1)S(1)}, bf16[1024,2,128]{0,2,1:T(8,128)(2,1)}, u32[]{:S(2)}) copy-start(bf16[1024,2,128]{0,2,1:T(8,128)(2,1)} %get-tuple-element.204) | copy-start | bytes 1572868 | tf_op jit(solution)/shard_map/while
  95.1 18.2 %all-to-all-start.3 = ((bf16[1024,2,128]{2,1,0:T(2,128)(2,1)}), bf16[1024,2,128]{2,1,0:T(2,128)(2,1)S(1)}, u32[]{:S(2)}, u32[]{:S(2)}) async-start(bf16[1024,2,128]{2,1,0:T(2,128)(2,1)} %copy.59), calls=%async_computation.3 | async-start | bytes 1048576 | tf_op jit(solution)/shard_map/all_to_all | solution.py:83
  113.6 4.8 %copy-start.4 = (bf16[1,128,2048]{2,1,0:T(8,128)(2,1)S(1)}, bf16[1,128,2048]{2,1,0:T(8,128)(2,1)}, u32[]{:S(2)}) copy-start(bf16[1,128,2048]{2,1,0:T(8,128)(2,1)} %param.25) | copy-start | bytes 1572868
  113.6 4.8 %copy-start.7 = (f32[2048]{0:T(1024)S(1)}, f32[2048]{0:T(1024)}, u32[]{:S(2)}) copy-start(f32[2048]{0:T(1024)} %param.27) | copy-start | bytes 24580
  113.7 5.2 %copy-start.8 = (f32[2048]{0:T(1024)S(1)}, f32[2048]{0:T(1024)}, u32[]{:S(2)}) copy-start(f32[2048]{0:T(1024)} %param.28) | copy-start | bytes 24580
  125.5 76.3 %copy-start.12 = (bf16[1,2048,512]{2,1,0:T(8,128)(2,1)S(1)}, bf16[1,2048,512]{2,1,0:T(8,128)(2,1)}, u32[]{:S(2)}) copy-start(bf16[1,2048,512]{2,1,0:T(8,128)(2,1)} %param.32) | copy-start | bytes 6291460
  200.1 1.7 copy-start.1
  212.9 4.0 %copy-start.11 = (f32[1,128,4]{1,2,0:T(4,128)S(1)}, f32[1,128,4]{1,2,0:T(4,128)}, u32[]{:S(2)}) copy-start(f32[1,128,4]{1,2,0:T(4,128)} %param.31) | copy-start | bytes 6148
  212.9 75.3 %all-to-all-start.5 = ((bf16[32,24,2048]{2,1,0:T(8,128)(2,1)}), bf16[32,24,2048]{2,1,0:T(8,128)(2,1)}, u32[]{:S(2)}, u32[]{:S(2)}) async-start(bf16[32,24,2048]{2,1,0:T(8,128)(2,1)} %bitcast.149), calls=%async_computation.5 | async-start | bytes 6291456 | tf_op jit(solution)/shard_map/all_to_all | solution.py:121
  306.8 4.4 %copy-start.9 = (f32[2048]{0:T(1024)S(1)}, f32[2048]{0:T(1024)}, u32[]{:S(2)}) copy-start(f32[2048]{0:T(1024)} %param.29) | copy-start | bytes 24580
where the time goes:
time: 315 us; the launch traced here: 313 us
  waiting for transfers between devices  110 us (35%)
  blocking collectives  74.6 us (24%)
  local copies, waits for them, and re-layouts  44.7 us (14%)
  matrix products  38.3 us (12%)
  starting transfers between devices  22.7 us (7%)
  other arithmetic  21.5 us (7%)
    all_to_all x1, blocking collectives, local(): lax.all_to_all(outgoing, ('sp', 'dp'), split_axis=0, concat_axis=0, tiled...  74.6 us
    all_to_all x1, waiting for transfers between devices, local(): lax.all_to_all(results, ('sp', 'dp'), split_axis=0, concat_axis=0, tiled=...  69.1 us
    sub x2, matrix products, one_block(): exponent = jnp.exp(scores - maxima)  14.3 us
    all_to_all x1, waiting for transfers between devices, local(): lax.all_to_all(value_vectors[0], 'sp', split_axis=1, concat_axis=0, tiled...  12.7 us
    all_to_all x1, waiting for transfers between devices, local(): lax.all_to_all(queries[0], 'sp', split_axis=1, concat_axis=0, tiled=True)  12.5 us
    dot_general x2, matrix products, feed_forward(): jnp.dot(hidden, down_w, preferred_element_type=jnp.float32)  12.5 us
    unnamed x31, local copies, waits for them, and re-layouts  8.84 us
    div x2, other arithmetic, one_block(): softmax_both = exponent / jnp.sum(exponent, axis=-1, keepdims=True)  7.91 us
  transfers between devices with their start and end apart: 5, of which 5 were waited for; matrix products, arithmetic and copies ran while one was open for 6% of the time, Pallas kernels for 0%

commit v1 on v0

v1 whole, which is shorter than its diff:
```python
import functools

import jax
import jax.numpy as jnp
from jax import lax
from jax.experimental import pallas as pl
from jax.experimental.pallas import tpu as pltpu
from jax.sharding import PartitionSpec as P

epsilon = 1e-06
MESH = pl.DeviceIdType.MESH
VMEM = pl.BlockSpec(memory_space=pltpu.VMEM)


def rms_scale(values_in, gain):
    return (
        values_in
        * lax.rsqrt(jnp.mean(values_in * values_in, axis=-1, keepdims=True) + epsilon)
        * gain
    )


def feed_forward(rows, gate_w, up_w, down_w):
    gate_val = jnp.dot(rows, gate_w, preferred_element_type=jnp.float32)
    up_val = jnp.dot(rows, up_w, preferred_element_type=jnp.float32)
    hidden = (jax.nn.silu(gate_val) * up_val).astype(jnp.bfloat16)
    return jnp.dot(hidden, down_w, preferred_element_type=jnp.float32).astype(jnp.bfloat16)


def columns_of(index, width):
    return pl.ds(pl.multiple_of(index * width, width), width)


def line_barrier(n, me):
    barrier = pltpu.get_barrier_semaphore()

    def greet(off, carry):
        pl.semaphore_signal(
            barrier, inc=1, device_id={"sp": lax.rem(me + off, n)}, device_id_type=MESH
        )
        return carry

    lax.fori_loop(1, n, greet, 0)
    pl.semaphore_wait(barrier, n - 1)


def to_heads_kernel(n, q_ref, k_ref, v_ref, qo_ref, ko_ref, vo_ref, send_sem, recv_sem, own_sem):
    me = lax.axis_index("sp")
    width = qo_ref.shape[2]
    pairs = ((q_ref, qo_ref), (k_ref, ko_ref), (v_ref, vo_ref))
    line_barrier(n, me)

    def copy(which, off):
        source, target = pairs[which]
        dst = lax.rem(me + off, n)
        return pltpu.make_async_remote_copy(
            src_ref=source.at[:, columns_of(dst, width)],
            dst_ref=target.at[me],
            send_sem=send_sem.at[which, off],
            recv_sem=recv_sem.at[which, off],
            device_id={"sp": dst},
            device_id_type=MESH,
        )

    def own(which):
        source, target = pairs[which]
        return pltpu.make_async_copy(
            source.at[:, columns_of(me, width)], target.at[me], own_sem.at[which]
        )

    def start(off, carry):
        for which in range(3):
            copy(which, off).start()
        return carry

    def finish(off, carry):
        for which in range(3):
            copy(which, off).wait()
        return carry

    lax.fori_loop(1, n, start, 0)
    for which in range(3):
        own(which).start()
    for which in range(3):
        own(which).wait()
    lax.fori_loop(1, n, finish, 0)


def to_heads(n, q, k, v):
    tok, model = q.shape
    width = model // n
    out = jax.ShapeDtypeStruct((n, tok, width), q.dtype)
    return pl.pallas_call(
        functools.partial(to_heads_kernel, n),
        out_shape=[out] * 3,
        in_specs=[VMEM] * 3,
        out_specs=[VMEM] * 3,
        scratch_shapes=[
            pltpu.SemaphoreType.DMA((3, n)),
            pltpu.SemaphoreType.DMA((3, n)),
            pltpu.SemaphoreType.DMA((3,)),
        ],
        compiler_params=pltpu.CompilerParams(
            collective_id=0, has_side_effects=True, vmem_limit_bytes=32 * 2**20
        ),
    )(q, k, v)


def to_tokens_kernel(n, a_ref, o_ref, send_sem, recv_sem, own_sem):
    me = lax.axis_index("sp")
    width = a_ref.shape[2]
    line_barrier(n, me)

    def copy(off):
        dst = lax.rem(me + off, n)
        return pltpu.make_async_remote_copy(
            src_ref=a_ref.at[dst],
            dst_ref=o_ref.at[:, columns_of(me, width)],
            send_sem=send_sem.at[off],
            recv_sem=recv_sem.at[off],
            device_id={"sp": dst},
            device_id_type=MESH,
        )

    def start(off, carry):
        copy(off).start()
        return carry

    def finish(off, carry):
        copy(off).wait()
        return carry

    lax.fori_loop(1, n, start, 0)
    own = pltpu.make_async_copy(a_ref.at[me], o_ref.at[:, columns_of(me, width)], own_sem)
    own.start()
    own.wait()
    lax.fori_loop(1, n, finish, 0)


def to_tokens(n, attended):
    _, tok, width = attended.shape
    return pl.pallas_call(
        functools.partial(to_tokens_kernel, n),
        out_shape=jax.ShapeDtypeStruct((tok, n * width), attended.dtype),
        in_specs=[VMEM],
        out_specs=VMEM,
        scratch_shapes=[
            pltpu.SemaphoreType.DMA((n,)),
            pltpu.SemaphoreType.DMA((n,)),
            pltpu.SemaphoreType.DMA,
        ],
        compiler_params=pltpu.CompilerParams(
            collective_id=1, has_side_effects=True, vmem_limit_bytes=32 * 2**20
        ),
    )(attended)


def attend_kernel(block, q_ref, k_ref, v_ref, lam_ref, gain_ref, o_ref):
    length, width = q_ref.shape
    value_size = gain_ref.shape[1]
    heads = width // value_size
    half = value_size // 2
    lane = lax.broadcasted_iota(jnp.int32, (block, value_size), 1)
    row = lax.broadcasted_iota(jnp.int32, (block, block), 0)
    col = lax.broadcasted_iota(jnp.int32, (block, block), 1)
    causal = col <= row
    contract = (((1,), (1,)), ((), ()))
    for head in range(heads):
        cols = slice(head * value_size, (head + 1) * value_size)
        for step in range(length // block):
            rows = slice(step * block, (step + 1) * block)
            past = step * block
            query = q_ref[rows, cols]
            near, far = [], []
            for which in range(2):
                keep = (lane < half) if which == 0 else (lane >= half)
                part = jnp.where(keep, query, jnp.zeros_like(query))
                s_near = lax.dot_general(
                    part, k_ref[rows, cols], contract, preferred_element_type=jnp.float32
                ) * (half**-0.5)
                s_near = jnp.where(causal, s_near, -jnp.inf)
                top = jnp.max(s_near, axis=-1, keepdims=True)
                if past:
                    s_far = lax.dot_general(
                        part, k_ref[:past, cols], contract, preferred_element_type=jnp.float32
                    ) * (half**-0.5)
                    top = jnp.maximum(top, jnp.max(s_far, axis=-1, keepdims=True))
                e_near = jnp.exp(s_near - top)
                total = jnp.sum(e_near, axis=-1, keepdims=True)
                if past:
                    e_far = jnp.exp(s_far - top)
                    total = total + jnp.sum(e_far, axis=-1, keepdims=True)
                scale = 1.0 / total
                if which == 1:
                    scale = scale * lam_ref[head]
                near.append(e_near * scale)
                if past:
                    far.append(e_far * scale)
            mixture = (near[0] - near[1]).astype(jnp.bfloat16)
            result = jnp.dot(mixture, v_ref[rows, cols], preferred_element_type=jnp.float32)
            if past:
                mixture = (far[0] - far[1]).astype(jnp.bfloat16)
                result += jnp.dot(
                    mixture, v_ref[:past, cols], preferred_element_type=jnp.float32
                )
            o_ref[rows, cols] = rms_scale(result, gain_ref[...]).astype(o_ref.dtype)


def attend(q, k, v, head_lambda, head_gain):
    return pl.pallas_call(
        functools.partial(attend_kernel, min(256, q.shape[0])),
        out_shape=jax.ShapeDtypeStruct(q.shape, q.dtype),
        in_specs=[VMEM] * 3 + [pl.BlockSpec(memory_space=pltpu.SMEM), VMEM],
        out_specs=VMEM,
        compiler_params=pltpu.CompilerParams(vmem_limit_bytes=48 * 2**20),
    )(q, k, v, head_lambda, head_gain.reshape(1, -1))


def half_place(sp_half, dp_size):
    sp, dp = lax.axis_index("sp"), lax.axis_index("dp")
    first = sp // sp_half * sp_half
    here = (sp - first) * dp_size + dp
    mirror = {"sp": lax.rem(sp + sp_half, 2 * sp_half), "dp": dp}

    def peer(place):
        return {"sp": first + place // dp_size, "dp": lax.rem(place, dp_size)}

    return here, mirror, peer


def half_barrier(group, here, mirror, peer):
    barrier = pltpu.get_barrier_semaphore()
    pl.semaphore_signal(barrier, inc=1, device_id=mirror, device_id_type=MESH)

    def greet(off, carry):
        pl.semaphore_signal(
            barrier, inc=1, device_id=peer(lax.rem(here + off, group)), device_id_type=MESH
        )
        return carry

    lax.fori_loop(1, group, greet, 0)
    pl.semaphore_wait(barrier, group)


def dispatch_kernel(
    sp_half,
    dp_size,
    own_ref,
    normed_ref,
    pick_ref,
    o_ref,
    tokens,
    rows,
    send_sem,
    recv_sem,
    far_send,
    far_recv,
    own_sem,
):
    group = sp_half * dp_size
    chunks, _, _, width = rows.shape
    here, mirror, peer = half_place(sp_half, dp_size)
    half_barrier(group, here, mirror, peer)

    def far(chunk):
        cols = pl.ds(chunk * width, width)
        return pltpu.make_async_remote_copy(
            src_ref=normed_ref.at[:, cols],
            dst_ref=tokens.at[chunk],
            send_sem=far_send.at[chunk],
            recv_sem=far_recv.at[chunk],
            device_id=mirror,
            device_id_type=MESH,
        )

    def near(off):
        place = lax.rem(here + off, group)
        return pltpu.make_async_remote_copy(
            src_ref=own_ref.at[place],
            dst_ref=o_ref.at[here],
            send_sem=send_sem.at[chunks, off],
            recv_sem=recv_sem.at[chunks, off],
            device_id=peer(place),
            device_id_type=MESH,
        )

    def passed(chunk, off):
        place = lax.rem(here + off, group)
        return pltpu.make_async_remote_copy(
            src_ref=rows.at[chunk, place],
            dst_ref=o_ref.at[group + here, :, pl.ds(chunk * width, width)],
            send_sem=send_sem.at[chunk, off],
            recv_sem=recv_sem.at[chunk, off],
            device_id=peer(place),
            device_id_type=MESH,
        )

    def over(action):
        lax.fori_loop(1, group, lambda off, carry: (action(off), carry)[1], 0)

    for chunk in range(chunks):
        far(chunk).start()
    over(lambda off: near(off).start())
    kept = pltpu.make_async_copy(own_ref.at[here], o_ref.at[here], own_sem.at[chunks])
    kept.start()
    for chunk in range(chunks):
        far(chunk).wait_recv()
        picked = jnp.dot(pick_ref[...], tokens[chunk], preferred_element_type=jnp.float32)
        rows[chunk] = picked.reshape(rows.shape[1:]).astype(rows.dtype)
        over(lambda off: passed(chunk, off).start())
        pltpu.make_async_copy(
            rows.at[chunk, here],
            o_ref.at[group + here, :, pl.ds(chunk * width, width)],
            own_sem.at[chunk],
        ).start()
    kept.wait()
    over(lambda off: near(off).wait())
    for chunk in range(chunks):
        far(chunk).wait_send()
        over(lambda off: passed(chunk, off).wait())
        pltpu.make_async_copy(
            rows.at[chunk, here],
            o_ref.at[group + here, :, pl.ds(chunk * width, width)],
            own_sem.at[chunk],
        ).wait()


def dispatch(sp_half, dp_size, own_rows, normed, pick_far, chunks):
    group, cap, model = own_rows.shape
    tok = normed.shape[0]
    width = model // chunks
    return pl.pallas_call(
        functools.partial(dispatch_kernel, sp_half, dp_size),
        out_shape=jax.ShapeDtypeStruct((2 * group, cap, model), normed.dtype),
        in_specs=[VMEM] * 3,
        out_specs=VMEM,
        scratch_shapes=[
            pltpu.VMEM((chunks, tok, width), normed.dtype),
            pltpu.VMEM((chunks, group, cap, width), normed.dtype),
            pltpu.SemaphoreType.DMA((chunks + 1, group)),
            pltpu.SemaphoreType.DMA((chunks + 1, group)),
            pltpu.SemaphoreType.DMA((chunks,)),
            pltpu.SemaphoreType.DMA((chunks,)),
            pltpu.SemaphoreType.DMA((chunks + 1,)),
        ],
        compiler_params=pltpu.CompilerParams(
            collective_id=2, has_side_effects=True, vmem_limit_bytes=40 * 2**20
        ),
    )(own_rows, normed, pick_far)


def collect_kernel(
    sp_half,
    dp_size,
    res_ref,
    high_ref,
    low_ref,
    o_ref,
    far_ref,
    landed,
    partial,
    send_sem,
    recv_sem,
    far_send,
    far_recv,
    own_sem,
):
    group = sp_half * dp_size
    chunks, _, cap, width = landed.shape
    here, mirror, peer = half_place(sp_half, dp_size)
    half_barrier(group, here, mirror, peer)

    def near(off):
        place = lax.rem(here + off, group)
        return pltpu.make_async_remote_copy(
            src_ref=res_ref.at[place],
            dst_ref=o_ref.at[here],
            send_sem=send_sem.at[chunks, off],
            recv_sem=recv_sem.at[chunks, off],
            device_id=peer(place),
            device_id_type=MESH,
        )

    def passed(chunk, off):
        place = lax.rem(here + off, group)
        return pltpu.make_async_remote_copy(
            src_ref=res_ref.at[group + place, :, pl.ds(chunk * width, width)],
            dst_ref=landed.at[chunk, here],
            send_sem=send_sem.at[chunk, off],
            recv_sem=recv_sem.at[chunk, off],
            device_id=peer(place),
            device_id_type=MESH,
        )

    def far(chunk):
        return pltpu.make_async_remote_copy(
            src_ref=partial.at[chunk],
            dst_ref=far_ref.at[:, pl.ds(chunk * width, width)],
            send_sem=far_send.at[chunk],
            recv_sem=far_recv.at[chunk],
            device_id=mirror,
            device_id_type=MESH,
        )

    def kept(chunk):
        return pltpu.make_async_copy(
            res_ref.at[group + here, :, pl.ds(chunk * width, width)],
            landed.at[chunk, here],
            own_sem.at[chunk],
        )

    def over(action):
        lax.fori_loop(1, group, lambda off, carry: (action(off), carry)[1], 0)

    for chunk in range(chunks):
        over(lambda off: passed(chunk, off).start())
        kept(chunk).start()
    over(lambda off: near(off).start())
    own = pltpu.make_async_copy(res_ref.at[here], o_ref.at[here], own_sem.at[chunks])
    own.start()
    contract = (((0,), (0,)), ((), ()))
    for chunk in range(chunks):
        kept(chunk).wait()
        over(lambda off: passed(chunk, off).wait_recv())
        block = landed[chunk].astype(jnp.float32).reshape(group * cap, width)
        block = block.astype(jnp.bfloat16)
        total = lax.dot_general(high_ref[...], block, contract, preferred_element_type=jnp.float32)
        total += lax.dot_general(low_ref[...], block, contract, preferred_element_type=jnp.float32)
        partial[chunk] = total.astype(partial.dtype)
        far(chunk).start()
    own.wait()
    over(lambda off: near(off).wait())
    for chunk in range(chunks):
        over(lambda off: passed(chunk, off).wait_send())
        far(chunk).wait()


def collect(sp_half, dp_size, results, high, low, chunks):
    twice, cap, model = results.shape
    group = twice // 2
    tok = high.shape[1]
    width = model // chunks
    return pl.pallas_call(
        functools.partial(collect_kernel, sp_half, dp_size),
        out_shape=[
            jax.ShapeDtypeStruct((group, cap, model), results.dtype),
            jax.ShapeDtypeStruct((tok, model), results.dtype),
        ],
        in_specs=[VMEM] * 3,
        out_specs=[VMEM] * 2,
        scratch_shapes=[
            pltpu.VMEM((chunks, group, cap, width), results.dtype),
            pltpu.VMEM((chunks, tok, width), results.dtype),
            pltpu.SemaphoreType.DMA((chunks + 1, group)),
            pltpu.SemaphoreType.DMA((chunks + 1, group)),
            pltpu.SemaphoreType.DMA((chunks,)),
            pltpu.SemaphoreType.DMA((chunks,)),
            pltpu.SemaphoreType.DMA((chunks + 1,)),
        ],
        compiler_params=pltpu.CompilerParams(
            collective_id=3, has_side_effects=True, vmem_limit_bytes=40 * 2**20
        ),
    )(results, high, low)


def slot_tables(chosen, weights, first, group, cap):
    tok = chosen.shape[0]
    ids = first + jnp.arange(group, dtype=jnp.int32)
    named = chosen.T[None] == ids[:, None, None]
    member = jnp.sum(named.astype(jnp.float32), axis=1)
    weight = jnp.sum(jnp.where(named, weights.T[None], 0.0), axis=1)
    before = jnp.arange(tok)[:, None] < jnp.arange(tok)[None, :]
    earlier = jnp.dot(
        member.astype(jnp.bfloat16),
        before.astype(jnp.bfloat16),
        preferred_element_type=jnp.float32,
    )
    rank = jnp.where(member > 0, earlier, -1.0)
    hit = rank[:, None, :] == jnp.arange(cap, dtype=jnp.float32)[None, :, None]
    spread = jnp.where(hit, weight[:, None, :], 0.0)
    high = spread.astype(jnp.bfloat16)
    low = (spread - high.astype(jnp.float32)).astype(jnp.bfloat16)
    flat = (group * cap, tok)
    return hit.astype(jnp.bfloat16).reshape(flat), high.reshape(flat), low.reshape(flat)


def local(
    queries,
    key_vectors,
    value_vectors,
    head_lambda,
    head_gain,
    residual,
    out_weight,
    mix_gain,
    pre_gain,
    post_gain,
    routes,
    route_weights,
    expert_gate,
    expert_up,
    expert_down,
    shared_gate,
    shared_up,
    shared_down,
):
    n, dp_size = lax.axis_size("sp"), lax.axis_size("dp")
    sp_half = n // 2
    group = sp_half * dp_size
    tok = queries.shape[1]
    top_count = routes.shape[2]
    cap = 3 * tok * top_count // (2 * n * dp_size)
    cap = (cap + 7) // 8 * 8
    model = residual.shape[2]
    chunks = 4

    sent = jnp.concatenate([routes[0].astype(jnp.float32), route_weights[0]], axis=1)
    far_sent = lax.ppermute(sent, "sp", [(i, (i + sp_half) % n) for i in range(n)])

    q, k, v = to_heads(
        n, queries.reshape(tok, -1), key_vectors.reshape(tok, -1), value_vectors.reshape(tok, -1)
    )
    width = q.shape[2]
    attended = attend(
        q.reshape(-1, width), k.reshape(-1, width), v.reshape(-1, width), head_lambda, head_gain
    )
    flat_heads = to_tokens(n, attended.reshape(n, tok, width))

    first = lax.axis_index("sp") // sp_half * group
    pick, high, low = slot_tables(routes[0], route_weights[0], first, group, cap)
    far_pick, far_high, far_low = slot_tables(
        far_sent[:, :top_count].astype(jnp.int32), far_sent[:, top_count:], first, group, cap
    )

    mixed_rows = jnp.dot(flat_heads, out_weight, preferred_element_type=jnp.float32)
    updated = (residual[0].astype(jnp.float32) + rms_scale(mixed_rows, mix_gain)).astype(
        jnp.bfloat16
    )
    normed = rms_scale(updated.astype(jnp.float32), pre_gain).astype(jnp.bfloat16)
    own_rows = jnp.dot(pick, normed, preferred_element_type=jnp.float32).astype(jnp.bfloat16)
    arrived = dispatch(
        sp_half, dp_size, own_rows.reshape(group, cap, model), normed, far_pick, chunks
    )
    shared_out = feed_forward(normed, shared_gate, shared_up, shared_down)
    results = feed_forward(
        arrived.reshape(-1, model), expert_gate[0], expert_up[0], expert_down[0]
    )
    returned, from_far = collect(
        sp_half, dp_size, results.reshape(2 * group, cap, model), far_high, far_low, chunks
    )
    rows = returned.reshape(group * cap, model)
    contract = (((0,), (0,)), ((), ()))
    routed = lax.dot_general(high, rows, contract, preferred_element_type=jnp.float32)
    routed += lax.dot_general(low, rows, contract, preferred_element_type=jnp.float32)
    combined = routed + from_far.astype(jnp.float32) + shared_out.astype(jnp.float32)
    output = (updated.astype(jnp.float32) + rms_scale(combined, post_gain)).astype(jnp.bfloat16)
    return output.reshape(1, tok, model)


def solution(mesh):
    in_specs = (
        P("dp", "sp", None, None),
        P("dp", "sp", None, None),
        P("dp", "sp", None, None),
        P("sp"),
        P(),
        P("dp", "sp", None),
        P(),
        P(),
        P(),
        P(),
        P("dp", "sp", None),
        P("dp", "sp", None),
        P(("sp", "dp"), None, None),
        P(("sp", "dp"), None, None),
        P(("sp", "dp"), None, None),
        P(),
        P(),
        P(),
    )
    out_specs = P("dp", "sp", None)
    return jax.shard_map(local, mesh=mesh, in_specs=in_specs, out_specs=out_specs, check_vma=False)
```

time: 315 us -> 207 us (0.66)
  Pallas kernels: 0 us -> 167 us
  waiting for transfers between devices: 110 us -> 0.01 us
  blocking collectives: 74.6 us -> 0 us
  local copies, waits for them, and re-layouts: 44.7 us -> 7.36 us
  starting transfers between devices: 22.7 us -> 4.06 us
  other arithmetic: 21.5 us -> 3.58 us
  matrix products: 38.3 us -> 24 us
    pallas_call x0 -> x5, Pallas kernels: none -> 167 us  [the longest x1 56.9 us: dispatch(): pl.pallas_call(functools.partial(dispatch_kernel, sp_half, dp_size), out_...]
    all_to_all x5 -> x0, waiting for transfers between devices: 110 us -> none  [the longest x1 69.1 us: local(): lax.all_to_all(results, ('sp', 'dp'), split_axis=0, concat_axis=0, tiled=...]
    all_to_all x1 -> x0, blocking collectives: 74.6 us -> none  [local(): lax.all_to_all(outgoing, ('sp', 'dp'), split_axis=0, concat_axis=0, tiled...]
    all_to_all x5 -> x0, starting transfers between devices: 22.7 us -> none  [the longest x1 7.31 us: local(): lax.all_to_all(queries[0], 'sp', split_axis=1, concat_axis=0, tiled=True)]
    sub x2 -> x0, matrix products: 14.3 us -> none  [one_block(): exponent = jnp.exp(scores - maxima)]
    gather x2 -> x0, local copies, waits for them, and re-layouts: 11.8 us -> none  [the longest x1 7.52 us: local(): picked = returned.reshape(experts_total * capacity, model_width)[slot_index]]
    div x2 -> x0, other arithmetic: 7.91 us -> none  [one_block(): softmax_both = exponent / jnp.sum(exponent, axis=-1, keepdims=True)]
    scatter x2 -> x0, local copies, waits for them, and re-layouts: 6.39 us -> none  [the longest x1 3.77 us: local(): occupied = jnp.zeros((experts_total * capacity,), jnp.bfloat16).at[slot_i...]
  transfers between devices with their start and end apart: 5 -> 1, of which waited for: 5 -> 0; matrix products, arithmetic and copies ran while one was open for 6% -> 7% of each run, Pallas kernels for 0% -> 27%
where the time goes in v1:
time: 207 us; the launch traced here: 206 us
  Pallas kernels  167 us (81%)
  matrix products  24 us (12%)
  local copies, waits for them, and re-layouts  7.36 us (4%)
  starting transfers between devices  4.06 us (2%)
  other arithmetic  3.58 us (2%)
    pallas_call x1, Pallas kernels, dispatch(): pl.pallas_call(functools.partial(dispatch_kernel, sp_half, dp_size), out_...  56.9 us
    pallas_call x1, Pallas kernels, collect(): pl.pallas_call(functools.partial(collect_kernel, sp_half, dp_size), out_s...  55 us
    pallas_call x1, Pallas kernels, to_heads(): pl.pallas_call(functools.partial(to_heads_kernel, n), out_shape=[out] * 3...  28.1 us
    pallas_call x1, Pallas kernels, to_tokens(): pl.pallas_call(functools.partial(to_tokens_kernel, n), out_shape=jax.Shap...  21.2 us
    dot_general x2, matrix products, feed_forward(): jnp.dot(hidden, down_w, preferred_element_type=jnp.float32)  12.3 us
    pallas_call x1, Pallas kernels, attend(): pl.pallas_call(functools.partial(attend_kernel, min(256, q.shape[0])), ou...  5.9 us
    unnamed x27, local copies, waits for them, and re-layouts  5.82 us
    dot_general x2, matrix products, feed_forward(): gate_val = jnp.dot(rows, gate_w, preferred_element_type=jnp.float32)  4.96 us
  transfers between devices with their start and end apart: 1, of which 0 were waited for; matrix products, arithmetic and copies ran while one was open for 7% of the time, Pallas kernels for 27%

profile of v1, /device:TPU:0, one launch (start us, length us, event | category | flops | bytes accessed | tf_op | source)
XLA Modules:
  0.0 206.3 jit_solution(6590222151595843054)
XLA Ops:
  0.0 0.0 copy-start
  0.0 0.8 bitcast_convert_fusion
  0.8 0.7 pad_maximum_fusion
  1.5 4.1 %collective-permute-start = (f32[128,8]{0,1:T(8,128)S(1)}, f32[128,8]{0,1:T(8,128)S(1)}, u32[]{:S(2)}, u32[]{:S(2)}) collective-permute-start(f32[128,8]{0,1:T(8,128)S(1)} %pad_maximum_fusion), channel_id=1, source_target_pairs={{0,16},{4,20},{8,24},{12,28},{16,0},{20,4},{24,8},{28,12},{1,17},{... | collective-permute-start | bytes 12296 | tf_op jit(solution)/shard_map/ppermute | solution.py:518
  5.6 1.2 copy.25
  6.8 0.0 copy-start.3
  6.8 0.0 copy-start.4
  6.8 1.4 copy_bitcast_fusion
  8.2 28.1 %shard_map.172 = (bf16[8,128,256]{2,1,0:T(8,128)(2,1)S(1)}, bf16[8,128,256]{2,1,0:T(8,128)(2,1)S(1)}, bf16[8,128,256]{2,1,0:T(8,128)(2,1)S(1)}) custom-call(bf16[128,2048]{1,0:T(8,128)(2,1)S(1)} %bitcast.100, bf16[128,2048]{1,0:T(8,128)(2,1)S(1)} %get-tuple-element.32.k_ref, bf16[128,2048]{1,0:T(8,128)(2,1)S(1)} %get-tuple-element.31.v_ref), custom_call_target="tpu_custom_call" | custom-call | tf_op jit(solution)/shard_map/pallas_call | solution.py:93
  36.3 0.0 copy-done.3
  36.3 0.0 copy-done.4
  36.3 5.9 %shard_map.173 = bf16[1024,256]{1,0:T(8,128)(2,1)S(1)} custom-call(bf16[1024,256]{1,0:T(8,128)(2,1)S(1)} %bitcast.102, bf16[1024,256]{1,0:T(8,128)(2,1)S(1)} %bitcast.103, bf16[1024,256]{1,0:T(8,128)(2,1)S(1)} %bitcast.104, f32[2]{0:T(128)S(1)} %copy-done.3, f32[1,128]{1,0:T(1,128)S(1)} %bitcast.105), custom_call_target="tpu_custom_call" | custom-call | tf_op jit(solution)/shard_map/pallas_call | solution.py:210
  42.2 21.2 %shard_map.174 = bf16[128,2048]{1,0:T(8,128)(2,1)S(1)} custom-call(bf16[8,128,256]{2,1,0:T(8,128)(2,1)S(1)} %bitcast.101), custom_call_target="tpu_custom_call" | custom-call | tf_op jit(solution)/shard_map/pallas_call | solution.py:142
  63.5 0.0 copy-start.6
  63.5 0.0 copy-start.7
  63.5 4.8 %multiply_reduce_fusion.1 = (f32[128]{0:T(128)S(1)}, f32[128,2048]{1,0:T(8,128)S(1)}) fusion(bf16[128,2048]{1,0:T(8,128)(2,1)S(1)} %shard_map.174, bf16[2048,2048]{1,0:T(8,128)(2,1)} %param.24), kind=kOutput, calls=%fused_computation.29 | convolution fusion | flops 1074265984 | bytes 9961984 | tf_op jit(solution)/shard_map/dot_general | solution.py:535
  68.3 0.0 copy-start.8
  68.3 0.0 copy-done.6
  68.3 0.0 copy-done.7
  68.3 0.4 fusion.12
  68.7 0.3 copy-done.8
  69.0 0.2 fusion.14.normed_ref
  69.2 2.0 fusion.49
  71.2 0.0 copy-start.10
  71.2 0.0 copy-start.11
  71.2 4.1 %fusion.3 = f32[128,2048]{1,0:T(8,128)} fusion(bf16[512,2048]{1,0:T(8,128)(2,1)} %param.35, bf16[128,2048]{1,0:T(8,128)(2,1)S(1)} %fusion.14.normed_ref, bf16[2048,512]{1,0:T(8,128)(2,1)} %param.34, f32[128,512]{1,0:T(8,128)S(1)} %fusion.49), kind=kOutput, calls=%fused_computation.8 | convolution fusion | flops 537788416 | bytes 6029312 | tf_op jit(solution)/shard_map/dot_general | solution.py:27
  75.4 0.1 eq.78
  75.5 0.0 collective-permute-done
  75.5 0.0 copy-done.10
  75.5 0.0 copy-done.11
  75.5 0.1 fusion.39
  75.6 0.1 convolution_select_fusion
  75.7 0.1 fusion.27.high_ref
  75.9 0.1 fusion.28.low_ref
  76.0 0.1 convolution_select_fusion.1
  76.1 0.1 fusion.29
  76.3 0.6 convolution_convert_fusion.1
  76.8 0.0 copy-start.12
  76.8 56.9 %shard_map.175 = bf16[32,24,2048]{2,1,0:T(8,128)(2,1)S(1)} custom-call(bf16[16,24,2048]{2,1,0:T(8,128)(2,1)S(1)} %bitcast.96, bf16[128,2048]{1,0:T(8,128)(2,1)S(1)} %fusion.14.normed_ref, bf16[384,128]{1,0:T(8,128)(2,1)S(1)} %get-tuple-element.25.pick_ref), custom_call_target="tpu_custom_call" | custom-call | tf_op jit(solution)/shard_map/pallas_call | solution.py:332
  133.7 0.0 copy-start.2
  133.8 1.6 copy-done.2
  135.4 0.0 copy-done.12
  135.4 2.9 %fusion.7 = f32[768,512]{1,0:T(8,128)} fusion(bf16[768,2048]{1,0:T(8,128)(2,1)S(1)} %bitcast.98, bf16[1,2048,512]{2,1,0:T(8,128)(2,1)S(1)} %copy-done.12), kind=kOutput, calls=%fused_computation.12 | convolution fusion | flops 1610612736 | bytes 6815744 | tf_op jit(solution)/shard_map/dot_general | solution.py:24
  138.3 0.0 copy-done
  138.3 8.1 %convolution_convert_fusion = bf16[768,2048]{1,0:T(8,128)(2,1)} fusion(bf16[1,512,2048]{2,1,0:T(8,128)(2,1)S(1)} %copy-done, f32[768,512]{1,0:T(8,128)} %fusion.7, bf16[768,2048]{1,0:T(8,128)(2,1)} %bitcast.99, bf16[1,2048,512]{2,1,0:T(8,128)(2,1)} %param.31), kind=kOutput, calls=%fused_computation | convolution fusion | flops 3225157632 | bytes 12058624 | tf_op jit(solution)/shard_map/dot_general | solution.py:27
  146.5 0.0 copy-start.1
  146.5 1.9 copy-done.1
  148.4 55.0 %shard_map.176 = (bf16[16,24,2048]{2,1,0:T(8,128)(2,1)S(1)}, bf16[128,2048]{1,0:T(8,128)(2,1)S(1)}) custom-call(bf16[32,24,2048]{2,1,0:T(8,128)(2,1)S(1)} %bitcast.97, bf16[384,128]{1,0:T(8,128)(2,1)S(1)} %fusion.27.high_ref, bf16[384,128]{1,0:T(8,128)(2,1)S(1)} %fusion.28.low_ref), custom_call_target="tpu_custom_call" | custom-call | tf_op jit(solution)/shard_map/pallas_call | solution.py:443
  203.4 0.0 copy-start.5
  203.4 0.5 convolution_bitcast_fusion
  203.9 0.7 copy-done.5
  204.6 0.0 copy-start.9
  204.6 0.6 multiply_reduce_fusion
  205.3 0.1 copy-done.9
  205.3 1.0 fusion.19
  (6 shorter events, 0.0 us)
Async XLA Ops:
  0.0 138.3 %copy-start = (bf16[1,512,2048]{2,1,0:T(8,128)(2,1)S(1)}, bf16[1,512,2048]{2,1,0:T(8,128)(2,1)}, u32[]{:S(2)}) copy-start(bf16[1,512,2048]{2,1,0:T(8,128)(2,1)} %param.32) | copy-start | bytes 6291460
  1.5 74.0 %collective-permute-start = (f32[128,8]{0,1:T(8,128)S(1)}, f32[128,8]{0,1:T(8,128)S(1)}, u32[]{:S(2)}, u32[]{:S(2)}) collective-permute-start(f32[128,8]{0,1:T(8,128)S(1)} %pad_maximum_fusion), channel_id=1, source_target_pairs={{0,16},{4,20},{8,24},{12,28},{16,0},{20,4},{24,8},{28,12},{1,17},{... | collective-permute-start | bytes 12296 | tf_op jit(solution)/shard_map/ppermute | solution.py:518
  6.8 29.5 %copy-start.3 = (f32[2]{0:T(128)S(1)}, f32[2]{0:T(128)}, u32[]{:S(2)}) copy-start(f32[2]{0:T(128)} %lam_ref.1) | copy-start | bytes 28
  6.8 29.5 %copy-start.4 = (f32[128]{0:T(128)S(1)}, f32[128]{0:T(128)}, u32[]{:S(2)}) copy-start(f32[128]{0:T(128)} %param.22) | copy-start | bytes 1540
  63.5 4.8 %copy-start.6 = (bf16[1,128,2048]{2,1,0:T(8,128)(2,1)S(1)}, bf16[1,128,2048]{2,1,0:T(8,128)(2,1)}, u32[]{:S(2)}) copy-start(bf16[1,128,2048]{2,1,0:T(8,128)(2,1)} %param.23) | copy-start | bytes 1572868
  63.5 4.8 %copy-start.7 = (f32[2048]{0:T(1024)S(1)}, f32[2048]{0:T(1024)}, u32[]{:S(2)}) copy-start(f32[2048]{0:T(1024)} %param.25) | copy-start | bytes 24580
  68.3 0.7 copy-start.8
  71.2 4.3 %copy-start.10 = (s32[1,128,4]{1,2,0:T(4,128)S(1)}, s32[1,128,4]{1,2,0:T(4,128)}, u32[]{:S(2)}) copy-start(s32[1,128,4]{1,2,0:T(4,128)} %param.28) | copy-start | bytes 6148
  71.2 4.3 %copy-start.11 = (f32[1,128,4]{1,2,0:T(4,128)S(1)}, f32[1,128,4]{1,2,0:T(4,128)}, u32[]{:S(2)}) copy-start(f32[1,128,4]{1,2,0:T(4,128)} %param.29) | copy-start | bytes 6148
  76.8 58.6 %copy-start.12 = (bf16[1,2048,512]{2,1,0:T(8,128)(2,1)S(1)}, bf16[1,2048,512]{2,1,0:T(8,128)(2,1)}, u32[]{:S(2)}) copy-start(bf16[1,2048,512]{2,1,0:T(8,128)(2,1)} %param.30) | copy-start | bytes 6291460
  133.7 1.7 copy-start.2
  146.5 1.9 copy-start.1
  203.4 1.2 copy-start.5
  204.6 0.7 copy-start.9

commit v2 on v1

--- a/solution.py
+++ b/solution.py
@@ -44,7 +44,22 @@
     pl.semaphore_wait(barrier, n - 1)
 
 
-def to_heads_kernel(n, q_ref, k_ref, v_ref, qo_ref, ko_ref, vo_ref, send_sem, recv_sem, own_sem):
+def to_heads_kernel(
+    n,
+    q_ref,
+    k_ref,
+    v_ref,
+    side_ref,
+    qo_ref,
+    ko_ref,
+    vo_ref,
+    side_out,
+    send_sem,
+    recv_sem,
+    own_sem,
+    side_send,
+    side_recv,
+):
     me = lax.axis_index("sp")
     width = qo_ref.shape[2]
     pairs = ((q_ref, qo_ref), (k_ref, ko_ref), (v_ref, vo_ref))
@@ -78,32 +93,44 @@
             copy(which, off).wait()
         return carry
 
+    side = pltpu.make_async_remote_copy(
+        src_ref=side_ref,
+        dst_ref=side_out,
+        send_sem=side_send,
+        recv_sem=side_recv,
+        device_id={"sp": lax.rem(me + n // 2, n)},
+        device_id_type=MESH,
+    )
     lax.fori_loop(1, n, start, 0)
+    side.start()
     for which in range(3):
         own(which).start()
     for which in range(3):
         own(which).wait()
     lax.fori_loop(1, n, finish, 0)
-
-
-def to_heads(n, q, k, v):
+    side.wait()
+
+
+def to_heads(n, q, k, v, side):
     tok, model = q.shape
     width = model // n
     out = jax.ShapeDtypeStruct((n, tok, width), q.dtype)
     return pl.pallas_call(
         functools.partial(to_heads_kernel, n),
-        out_shape=[out] * 3,
-        in_specs=[VMEM] * 3,
-        out_specs=[VMEM] * 3,
+        out_shape=[out] * 3 + [jax.ShapeDtypeStruct(side.shape, side.dtype)],
+        in_specs=[VMEM] * 4,
+        out_specs=[VMEM] * 4,
         scratch_shapes=[
             pltpu.SemaphoreType.DMA((3, n)),
             pltpu.SemaphoreType.DMA((3, n)),
             pltpu.SemaphoreType.DMA((3,)),
+            pltpu.SemaphoreType.DMA,
+            pltpu.SemaphoreType.DMA,
         ],
         compiler_params=pltpu.CompilerParams(
             collective_id=0, has_side_effects=True, vmem_limit_bytes=32 * 2**20
         ),
-    )(q, k, v)
+    )(q, k, v, side)
 
 
 def to_tokens_kernel(n, a_ref, o_ref, send_sem, recv_sem, own_sem):
@@ -242,225 +269,225 @@
     pl.semaphore_wait(barrier, group)
 
 
-def dispatch_kernel(
+def experts_kernel(
     sp_half,
     dp_size,
-    own_ref,
     normed_ref,
-    pick_ref,
+    own_pick_ref,
+    far_pick_ref,
+    high_ref,
+    low_ref,
+    gate_hbm,
+    up_hbm,
+    down_hbm,
     o_ref,
+    far_ref,
+    gate_w,
+    up_w,
+    down_w,
+    own_rows,
     tokens,
     rows,
-    send_sem,
-    recv_sem,
-    far_send,
-    far_recv,
-    own_sem,
-):
-    group = sp_half * dp_size
-    chunks, _, _, width = rows.shape
-    here, mirror, peer = half_place(sp_half, dp_size)
-    half_barrier(group, here, mirror, peer)
-
-    def far(chunk):
-        cols = pl.ds(chunk * width, width)
-        return pltpu.make_async_remote_copy(
-            src_ref=normed_ref.at[:, cols],
-            dst_ref=tokens.at[chunk],
-            send_sem=far_send.at[chunk],
-            recv_sem=far_recv.at[chunk],
-            device_id=mirror,
-            device_id_type=MESH,
-        )
-
-    def near(off):
-        place = lax.rem(here + off, group)
-        return pltpu.make_async_remote_copy(
-            src_ref=own_ref.at[place],
-            dst_ref=o_ref.at[here],
-            send_sem=send_sem.at[chunks, off],
-            recv_sem=recv_sem.at[chunks, off],
-            device_id=peer(place),
-            device_id_type=MESH,
-        )
-
-    def passed(chunk, off):
-        place = lax.rem(here + off, group)
-        return pltpu.make_async_remote_copy(
-            src_ref=rows.at[chunk, place],
-            dst_ref=o_ref.at[group + here, :, pl.ds(chunk * width, width)],
-            send_sem=send_sem.at[chunk, off],
-            recv_sem=recv_sem.at[chunk, off],
-            device_id=peer(place),
-            device_id_type=MESH,
-        )
-
-    def over(action):
-        lax.fori_loop(1, group, lambda off, carry: (action(off), carry)[1], 0)
-
-    for chunk in range(chunks):
-        far(chunk).start()
-    over(lambda off: near(off).start())
-    kept = pltpu.make_async_copy(own_ref.at[here], o_ref.at[here], own_sem.at[chunks])
-    kept.start()
-    for chunk in range(chunks):
-        far(chunk).wait_recv()
-        picked = jnp.dot(pick_ref[...], tokens[chunk], preferred_element_type=jnp.float32)
-        rows[chunk] = picked.reshape(rows.shape[1:]).astype(rows.dtype)
-        over(lambda off: passed(chunk, off).start())
-        pltpu.make_async_copy(
-            rows.at[chunk, here],
-            o_ref.at[group + here, :, pl.ds(chunk * width, width)],
-            own_sem.at[chunk],
-        ).start()
-    kept.wait()
-    over(lambda off: near(off).wait())
-    for chunk in range(chunks):
-        far(chunk).wait_send()
-        over(lambda off: passed(chunk, off).wait())
-        pltpu.make_async_copy(
-            rows.at[chunk, here],
-            o_ref.at[group + here, :, pl.ds(chunk * width, width)],
-            own_sem.at[chunk],
-        ).wait()
-
-
-def dispatch(sp_half, dp_size, own_rows, normed, pick_far, chunks):
-    group, cap, model = own_rows.shape
-    tok = normed.shape[0]
-    width = model // chunks
-    return pl.pallas_call(
-        functools.partial(dispatch_kernel, sp_half, dp_size),
-        out_shape=jax.ShapeDtypeStruct((2 * group, cap, model), normed.dtype),
-        in_specs=[VMEM] * 3,
-        out_specs=VMEM,
-        scratch_shapes=[
-            pltpu.VMEM((chunks, tok, width), normed.dtype),
-            pltpu.VMEM((chunks, group, cap, width), normed.dtype),
-            pltpu.SemaphoreType.DMA((chunks + 1, group)),
-            pltpu.SemaphoreType.DMA((chunks + 1, group)),
-            pltpu.SemaphoreType.DMA((chunks,)),
-            pltpu.SemaphoreType.DMA((chunks,)),
-            pltpu.SemaphoreType.DMA((chunks + 1,)),
-        ],
-        compiler_params=pltpu.CompilerParams(
-            collective_id=2, has_side_effects=True, vmem_limit_bytes=40 * 2**20
-        ),
-    )(own_rows, normed, pick_far)
-
-
-def collect_kernel(
-    sp_half,
-    dp_size,
-    res_ref,
-    high_ref,
-    low_ref,
-    o_ref,
-    far_ref,
+    own_in,
+    far_in,
+    flat,
+    hidden,
+    own_out,
+    far_out,
     landed,
     partial,
     send_sem,
     recv_sem,
+    back_send,
+    back_recv,
     far_send,
     far_recv,
-    own_sem,
+    local_sem,
 ):
     group = sp_half * dp_size
-    chunks, _, cap, width = landed.shape
+    chunks, _, cap, width = rows.shape
     here, mirror, peer = half_place(sp_half, dp_size)
     half_barrier(group, here, mirror, peer)
 
-    def near(off):
+    def cols(chunk):
+        return pl.ds(chunk * width, width)
+
+    def far(way, chunk):
+        return pltpu.make_async_remote_copy(
+            src_ref=(partial.at[chunk] if way else normed_ref.at[:, cols(chunk)]),
+            dst_ref=(far_ref.at[:, cols(chunk)] if way else tokens.at[chunk]),
+            send_sem=far_send.at[way, chunk],
+            recv_sem=far_recv.at[way, chunk],
+            device_id=mirror,
+            device_id_type=MESH,
+        )
+
+    def send(off, source, target, row, sends, recvs):
         place = lax.rem(here + off, group)
         return pltpu.make_async_remote_copy(
-            src_ref=res_ref.at[place],
-            dst_ref=o_ref.at[here],
-            send_sem=send_sem.at[chunks, off],
-            recv_sem=recv_sem.at[chunks, off],
+            src_ref=source(place),
+            dst_ref=target(here),
+            send_sem=sends.at[row, off],
+            recv_sem=recvs.at[row, off],
             device_id=peer(place),
             device_id_type=MESH,
         )
 
-    def passed(chunk, off):
-        place = lax.rem(here + off, group)
-        return pltpu.make_async_remote_copy(
-            src_ref=res_ref.at[group + place, :, pl.ds(chunk * width, width)],
-            dst_ref=landed.at[chunk, here],
-            send_sem=send_sem.at[chunk, off],
-            recv_sem=recv_sem.at[chunk, off],
-            device_id=peer(place),
-            device_id_type=MESH,
-        )
-
-    def far(chunk):
-        return pltpu.make_async_remote_copy(
-            src_ref=partial.at[chunk],
-            dst_ref=far_ref.at[:, pl.ds(chunk * width, width)],
-            send_sem=far_send.at[chunk],
-            recv_sem=far_recv.at[chunk],
-            device_id=mirror,
-            device_id_type=MESH,
-        )
-
-    def kept(chunk):
-        return pltpu.make_async_copy(
-            res_ref.at[group + here, :, pl.ds(chunk * width, width)],
-            landed.at[chunk, here],
-            own_sem.at[chunk],
-        )
+    def keep(source, target, index):
+        return pltpu.make_async_copy(source(here), target(here), local_sem.at[index])
 
     def over(action):
         lax.fori_loop(1, group, lambda off, carry: (action(off), carry)[1], 0)
 
-    for chunk in range(chunks):
+    out_own = (lambda p: own_rows.at[p], lambda p: own_in.at[p])
+    back_own = (lambda p: own_out.at[p], lambda p: o_ref.at[p])
+
+    def out_far(chunk):
+        return (lambda p: rows.at[chunk, p], lambda p: far_in.at[p, :, cols(chunk)])
+
+    def back_far(chunk):
+        return (lambda p: far_out.at[p, :, cols(chunk)], lambda p: landed.at[chunk, p])
+
+    def near(off):
+        return send(off, *out_own, chunks, send_sem, recv_sem)
+
+    def passed(chunk, off):
+        return send(off, *out_far(chunk), chunk, send_sem, recv_sem)
+
+    def near_back(off):
+        return send(off, *back_own, chunks, back_send, back_recv)
+
+    def passed_back(chunk, off):
+        return send(off, *back_far(chunk), chunk, back_send, back_recv)
+
+    loads = [
+        pltpu.make_async_copy(source, target, local_sem.at[2 * chunks + 2 + index])
+        for index, (source, target) in enumerate(
+            ((gate_hbm, gate_w), (up_hbm, up_w), (down_hbm, down_w))
+        )
+    ]
+    tile = min(256, gate_w.shape[1])
+
+    def hidden_of(block):
+        for chunk in range(chunks):
+            part = block[:, :, chunk * width : (chunk + 1) * width].astype(jnp.float32)
+            flat[:, chunk * width : (chunk + 1) * width] = part.reshape(
+                group * cap, width
+            ).astype(flat.dtype)
+
+        def one(index, carry):
+            some = columns_of(index, tile)
+            gate_val = jnp.dot(flat[...], gate_w[:, some], preferred_element_type=jnp.float32)
+            up_val = jnp.dot(flat[...], up_w[:, some], preferred_element_type=jnp.float32)
+            hidden[:, some] = (jax.nn.silu(gate_val) * up_val).astype(hidden.dtype)
+            return carry
+
+        lax.fori_loop(0, gate_w.shape[1] // tile, one, 0)
+
+    def down_to(target, chunk):
+        part = slice(chunk * width, (chunk + 1) * width)
+        value = jnp.dot(hidden[...], down_w[:, part], preferred_element_type=jnp.float32)
+        target[:, :, part] = value.reshape(group, cap, width).astype(target.dtype)
+
+    for chunk in range(chunks):
+        far(0, chunk).start()
+    for chunk in range(chunks):
+        part = slice(chunk * width, (chunk + 1) * width)
+        value = jnp.dot(
+            own_pick_ref[...], normed_ref[:, part], preferred_element_type=jnp.float32
+        )
+        own_rows[:, :, part] = value.reshape(group, cap, width).astype(own_rows.dtype)
+    over(lambda off: near(off).start())
+    keep(*out_own, 2 * chunks).start()
+    for load in loads:
+        load.start()
+    for chunk in range(chunks):
+        far(0, chunk).wait_recv()
+        picked = jnp.dot(far_pick_ref[...], tokens[chunk], preferred_element_type=jnp.float32)
+        rows[chunk] = picked.reshape(rows.shape[1:]).astype(rows.dtype)
         over(lambda off: passed(chunk, off).start())
-        kept(chunk).start()
-    over(lambda off: near(off).start())
-    own = pltpu.make_async_copy(res_ref.at[here], o_ref.at[here], own_sem.at[chunks])
-    own.start()
+        keep(*out_far(chunk), chunk).start()
+
+    for load in loads:
+        load.wait()
+    keep(*out_own, 2 * chunks).wait()
+    over(lambda off: near(off).wait_recv())
+    hidden_of(own_in)
+    for chunk in range(chunks):
+        down_to(own_out, chunk)
+    over(lambda off: near_back(off).start())
+    keep(*back_own, 2 * chunks + 1).start()
+
+    for chunk in range(chunks):
+        keep(*out_far(chunk), chunk).wait()
+        over(lambda off: passed(chunk, off).wait_recv())
+    hidden_of(far_in)
+    for chunk in range(chunks):
+        down_to(far_out, chunk)
+        over(lambda off: passed_back(chunk, off).start())
+        keep(*back_far(chunk), chunks + chunk).start()
+
     contract = (((0,), (0,)), ((), ()))
     for chunk in range(chunks):
-        kept(chunk).wait()
-        over(lambda off: passed(chunk, off).wait_recv())
+        keep(*back_far(chunk), chunks + chunk).wait()
+        over(lambda off: passed_back(chunk, off).wait_recv())
         block = landed[chunk].astype(jnp.float32).reshape(group * cap, width)
         block = block.astype(jnp.bfloat16)
         total = lax.dot_general(high_ref[...], block, contract, preferred_element_type=jnp.float32)
         total += lax.dot_general(low_ref[...], block, contract, preferred_element_type=jnp.float32)
         partial[chunk] = total.astype(partial.dtype)
-        far(chunk).start()
-    own.wait()
-    over(lambda off: near(off).wait())
+        far(1, chunk).start()
+
+    keep(*back_own, 2 * chunks + 1).wait()
+    over(lambda off: near(off).wait_send())
+    over(lambda off: near_back(off).wait())
     for chunk in range(chunks):
         over(lambda off: passed(chunk, off).wait_send())
-        far(chunk).wait()
-
-
-def collect(sp_half, dp_size, results, high, low, chunks):
-    twice, cap, model = results.shape
-    group = twice // 2
-    tok = high.shape[1]
+        over(lambda off: passed_back(chunk, off).wait_send())
+        far(0, chunk).wait_send()
+        far(1, chunk).wait()
+
+
+def run_experts(sp_half, dp_size, cap, chunks, normed, picks, parts, gate, up, down):
+    group = sp_half * dp_size
+    tok, model = normed.shape
+    ff = gate.shape[1]
     width = model // chunks
+    kind = normed.dtype
+    whole = pltpu.VMEM((group, cap, model), kind)
+    pieces = pltpu.VMEM((chunks, group, cap, width), kind)
+    token_pieces = pltpu.VMEM((chunks, tok, width), kind)
     return pl.pallas_call(
-        functools.partial(collect_kernel, sp_half, dp_size),
+        functools.partial(experts_kernel, sp_half, dp_size),
         out_shape=[
-            jax.ShapeDtypeStruct((group, cap, model), results.dtype),
-            jax.ShapeDtypeStruct((tok, model), results.dtype),
+            jax.ShapeDtypeStruct((group, cap, model), kind),
+            jax.ShapeDtypeStruct((tok, model), kind),
         ],
-        in_specs=[VMEM] * 3,
+        in_specs=[VMEM] * 5 + [pl.BlockSpec(memory_space=pl.ANY)] * 3,
         out_specs=[VMEM] * 2,
         scratch_shapes=[
-            pltpu.VMEM((chunks, group, cap, width), results.dtype),
-            pltpu.VMEM((chunks, tok, width), results.dtype),
-            pltpu.SemaphoreType.DMA((chunks + 1, group)),
-            pltpu.SemaphoreType.DMA((chunks + 1, group)),
-            pltpu.SemaphoreType.DMA((chunks,)),
-            pltpu.SemaphoreType.DMA((chunks,)),
-            pltpu.SemaphoreType.DMA((chunks + 1,)),
-        ],
+            pltpu.VMEM((model, ff), kind),
+            pltpu.VMEM((model, ff), kind),
+            pltpu.VMEM((ff, model), kind),
+            whole,
+            token_pieces,
+            pieces,
+            whole,
+            whole,
+            pltpu.VMEM((group * cap, model), kind),
+            pltpu.VMEM((group * cap, ff), kind),
+            whole,
+            whole,
+            pieces,
+            token_pieces,
+        ]
+        + [pltpu.SemaphoreType.DMA((chunks + 1, group))] * 4
+        + [pltpu.SemaphoreType.DMA((2, chunks))] * 2
+        + [pltpu.SemaphoreType.DMA((2 * chunks + 5,))],
         compiler_params=pltpu.CompilerParams(
-            collective_id=3, has_side_effects=True, vmem_limit_bytes=40 * 2**20
+            collective_id=2, has_side_effects=True, vmem_limit_bytes=56 * 2**20
         ),
-    )(results, high, low)
+    )(normed, *picks, *parts, gate, up, down)
 
 
 def slot_tables(chosen, weights, first, group, cap):
@@ -515,10 +542,14 @@
     chunks = 4
 
     sent = jnp.concatenate([routes[0].astype(jnp.float32), route_weights[0]], axis=1)
-    far_sent = lax.ppermute(sent, "sp", [(i, (i + sp_half) % n) for i in range(n)])
-
-    q, k, v = to_heads(
-        n, queries.reshape(tok, -1), key_vectors.reshape(tok, -1), value_vectors.reshape(tok, -1)
+    sent = jnp.pad(sent, ((0, 0), (0, 128 - 2 * top_count)))
+
+    q, k, v, far_sent = to_heads(
+        n,
+        queries.reshape(tok, -1),
+        key_vectors.reshape(tok, -1),
+        value_vectors.reshape(tok, -1),
+        sent,
     )
     width = q.shape[2]
     attended = attend(
@@ -529,7 +560,7 @@
     first = lax.axis_index("sp") // sp_half * group
     pick, high, low = slot_tables(routes[0], route_weights[0], first, group, cap)
     far_pick, far_high, far_low = slot_tables(
-        far_sent[:, :top_count].astype(jnp.int32), far_sent[:, top_count:], first, group, cap
+        far_sent[:, :top_count].astype(jnp.int32), far_sent[:, top_count : 2 * top_count], first, group, cap
     )
 
     mixed_rows = jnp.dot(flat_heads, out_weight, preferred_element_type=jnp.float32)
@@ -537,17 +568,19 @@
         jnp.bfloat16
     )
     normed = rms_scale(updated.astype(jnp.float32), pre_gain).astype(jnp.bfloat16)
-    own_rows = jnp.dot(pick, normed, preferred_element_type=jnp.float32).astype(jnp.bfloat16)
-    arrived = dispatch(
-        sp_half, dp_size, own_rows.reshape(group, cap, model), normed, far_pick, chunks
+    returned, from_far = run_experts(
+        sp_half,
+        dp_size,
+        cap,
+        chunks,
+        normed,
+        (pick, far_pick),
+        (far_high, far_low),
+        expert_gate[0],
+        expert_up[0],
+        expert_down[0],
     )
     shared_out = feed_forward(normed, shared_gate, shared_up, shared_down)
-    results = feed_forward(
-        arrived.reshape(-1, model), expert_gate[0], expert_up[0], expert_down[0]
-    )
-    returned, from_far = collect(
-        sp_half, dp_size, results.reshape(2 * group, cap, model), far_high, far_low, chunks
-    )
     rows = returned.reshape(group * cap, model)
     contract = (((0,), (0,)), ((), ()))
     routed = lax.dot_general(high, rows, contract, preferred_element_type=jnp.float32)

time: 207 us -> 199 us (0.961); the launches traced: 206 us -> 195 us
  matrix products: 24 us -> 12.6 us
  Pallas kernels: 167 us -> 173 us
  starting transfers between devices: 4.06 us -> 0 us
  local copies, waits for them, and re-layouts: 7.36 us -> 4.11 us
    pallas_call x1, Pallas kernels: 28.1 us -> 44.1 us  [to_heads(): pl.pallas_call(functools.partial(to_heads_kernel, n), out_shape=[out] * 3...]
    dot_general x2 -> x1, matrix products: 12.3 us -> 3.39 us  [feed_forward(): jnp.dot(hidden, down_w, preferred_element_type=jnp.float32)]
    pallas_call x1, Pallas kernels: 21.2 us -> 12.6 us  [to_tokens(): pl.pallas_call(functools.partial(to_tokens_kernel, n), out_shape=jax.Shap...]
    dot_general x2 -> x1, matrix products: 4.96 us -> 0.45 us  [feed_forward(): gate_val = jnp.dot(rows, gate_w, preferred_element_type=jnp.float32)]
    ppermute x1 -> x0, starting transfers between devices: 4.06 us -> none  [local(): lax.ppermute(sent, 'sp', [(i, (i + sp_half) % n) for i in range(n)])]
    unnamed x27, local copies, waits for them, and re-layouts: 5.82 us -> 2.32 us
    pallas_call x2 -> x1, Pallas kernels: 112 us -> 110 us  [run_experts(): pl.pallas_call(functools.partial(experts_kernel, sp_half, dp_size), out_s...]
  transfers between devices with their start and end apart: 1 -> 0, of which waited for: 0 -> 0; matrix products, arithmetic and copies ran while one was open for 7% -> 0% of each run, Pallas kernels for 27% -> 0%
where the time goes in v2:
time: 199 us; the launch traced here: 195 us
  Pallas kernels  173 us (87%)
  matrix products  12.6 us (6%)
  other arithmetic  5.63 us (3%)
  local copies, waits for them, and re-layouts  4.11 us (2%)
    pallas_call x1, Pallas kernels, run_experts(): pl.pallas_call(functools.partial(experts_kernel, sp_half, dp_size), out_s...  110 us
    pallas_call x1, Pallas kernels, to_heads(): pl.pallas_call(functools.partial(to_heads_kernel, n), out_shape=[out] * 3...  44.1 us
    pallas_call x1, Pallas kernels, to_tokens(): pl.pallas_call(functools.partial(to_tokens_kernel, n), out_shape=jax.Shap...  12.6 us
    pallas_call x1, Pallas kernels, attend(): pl.pallas_call(functools.partial(attend_kernel, min(256, q.shape[0])), ou...  5.9 us
    dot_general x1, matrix products, local(): jnp.dot(flat_heads, out_weight, preferred_element_type=jnp.float32)  4.78 us

profile of v2, /device:TPU:0, one launch (start us, length us, event | category | flops | bytes accessed | tf_op | source)
XLA Modules:
  0.0 195.3 jit_solution(17538207726483506085)
XLA Ops:
  0.0 0.0 copy-start
  0.0 0.8 bitcast_convert_fusion
  0.8 0.7 pad_maximum_fusion
  1.5 0.1 eq.78
  1.6 0.1 copy.28
  1.7 1.2 copy.37
  2.9 0.0 copy-start.1
  2.9 0.0 copy-start.2
  2.9 1.4 copy_bitcast_fusion
  4.4 44.1 %shard_map.172 = (bf16[8,128,256]{2,1,0:T(8,128)(2,1)S(1)}, bf16[8,128,256]{2,1,0:T(8,128)(2,1)S(1)}, bf16[8,128,256]{2,1,0:T(8,128)(2,1)S(1)}, f32[128,128]{1,0:T(8,128)S(1)}) custom-call(bf16[128,2048]{1,0:T(8,128)(2,1)S(1)} %bitcast.81, bf16[128,2048]{1,0:T(8,128)(2,1)S(1)} %get-tuple-element.34.k_ref, bf16[128,2048]{1,0:T(8,128)(2,1)S(1)} %get-tuple-element.33.v_ref, ...), custom_call_target="tpu_custom_call" | custom-call | tf_op jit(solution)/shard_map/pallas_call | solution.py:118
  48.5 0.0 copy-start.11
  48.5 0.0 copy-start.12
  48.5 0.0 copy-done.1
  48.6 0.0 copy-done.2
  48.6 5.9 %shard_map.173 = bf16[1024,256]{1,0:T(8,128)(2,1)S(1)} custom-call(bf16[1024,256]{1,0:T(8,128)(2,1)S(1)} %bitcast.83, bf16[1024,256]{1,0:T(8,128)(2,1)S(1)} %bitcast.84, bf16[1024,256]{1,0:T(8,128)(2,1)S(1)} %bitcast.85, f32[2]{0:T(128)S(1)} %copy-done.1, f32[1,128]{1,0:T(1,128)S(1)} %bitcast.86), custom_call_target="tpu_custom_call" | custom-call | tf_op jit(solution)/shard_map/pallas_call | solution.py:237
  54.5 12.6 %shard_map.174 = bf16[128,2048]{1,0:T(8,128)(2,1)S(1)} custom-call(bf16[8,128,256]{2,1,0:T(8,128)(2,1)S(1)} %bitcast.82), custom_call_target="tpu_custom_call" | custom-call | tf_op jit(solution)/shard_map/pallas_call | solution.py:169
  67.1 0.1 slice_bitcast_fusion
  67.2 0.1 copy.30
  67.3 0.1 copy.29
  67.3 0.0 copy-done.11
  67.3 0.0 copy-done.12
  67.3 0.1 fusion.31
  67.5 0.1 convolution_select_fusion.1
  67.6 0.1 convolution_select_fusion
  67.7 0.8 fusion.19.low_ref
  68.5 0.7 fusion.18.high_ref
  69.2 0.8 fusion.20
  70.0 0.0 copy-start.7
  70.0 0.0 copy-start.8
  70.0 4.8 %multiply_reduce_fusion.1 = (f32[128]{0:T(128)S(1)}, f32[128,2048]{1,0:T(8,128)S(1)}) fusion(bf16[128,2048]{1,0:T(8,128)(2,1)S(1)} %shard_map.174, bf16[2048,2048]{1,0:T(8,128)(2,1)} %param.24), kind=kOutput, calls=%fused_computation.21 | convolution fusion | flops 1074265984 | bytes 9961984 | tf_op jit(solution)/shard_map/dot_general | solution.py:566
  74.8 0.0 copy-start.9
  74.8 0.0 copy-start.6
  74.9 0.0 copy-done.7
  74.9 0.0 copy-done.8
  74.9 0.4 fusion.5
  75.3 0.3 copy-done.9
  75.5 0.2 fusion.7.normed_ref
  75.7 0.7 copy-done.6
  76.4 0.0 copy-start.3
  76.4 0.4 fusion.40
  76.9 0.0 copy-done
  76.9 3.4 %fusion.3 = f32[128,2048]{1,0:T(8,128)} fusion(bf16[512,2048]{1,0:T(8,128)(2,1)S(1)} %copy-done, bf16[128,2048]{1,0:T(8,128)(2,1)S(1)} %fusion.7.normed_ref, bf16[2048,512]{1,0:T(8,128)(2,1)} %param.34, f32[128,512]{1,0:T(8,128)S(1)} %fusion.40), kind=kOutput, calls=%fused_computation.6 | convolution fusion | flops 537788416 | bytes 6029312 | tf_op jit(solution)/shard_map/dot_general | solution.py:27
  80.3 0.0 copy-done.3
  80.3 110.1 %shard_map.175 = (bf16[16,24,2048]{2,1,0:T(8,128)(2,1)}, bf16[128,2048]{1,0:T(8,128)(2,1)}) custom-call(bf16[128,2048]{1,0:T(8,128)(2,1)} %copy-done.3, bf16[384,128]{1,0:T(8,128)(2,1)} %get-tuple-element.28.own_pick_ref, bf16[384,128]{1,0:T(8,128)(2,1)} %get-tuple-element.27.far_pick_ref, bf16[384,128]{1,0:T(8,128)(2,1)} %fusion.18.high_ref, ...), custom_call_target="tpu_custom_call" | custom-call | tf_op jit(solution)/shard_map/pallas_call | solution.py:460
  190.4 0.0 copy-start.4
  190.4 0.0 copy-start.5
  190.4 2.0 %convolution_bitcast_fusion = f32[128,2048]{1,0:T(8,128)S(1)} fusion(bf16[16,24,2048]{2,1,0:T(8,128)(2,1)} %get-tuple-element.15, f32[16,128]{1,0:T(8,128)S(1)} %get-tuple-element.17, f32[16,128]{1,0:T(8,128)S(1)} %convolution_select_fusion.1), kind=kOutput, calls=%fused_computation | convolution fusion | flops 201621504 | bytes 2637824 | tf_op jit(solution)/shard_map/dot_general | solution.py:587
  192.4 0.0 copy-done.4
  192.4 0.1 copy-done.5
  192.5 0.0 copy-start.10
  192.5 1.7 multiply_reduce_fusion
  194.2 0.0 copy-done.10
  194.2 1.0 fusion.10
  (6 shorter events, 0.0 us)
Async XLA Ops:
  0.0 76.9 %copy-start = (bf16[512,2048]{1,0:T(8,128)(2,1)S(1)}, bf16[512,2048]{1,0:T(8,128)(2,1)}, u32[]{:S(2)}) copy-start(bf16[512,2048]{1,0:T(8,128)(2,1)} %param.35) | copy-start | bytes 6291460
  2.9 45.6 %copy-start.1 = (f32[2]{0:T(128)S(1)}, f32[2]{0:T(128)}, u32[]{:S(2)}) copy-start(f32[2]{0:T(128)} %lam_ref.1) | copy-start | bytes 28
  2.9 45.6 %copy-start.2 = (f32[128]{0:T(128)S(1)}, f32[128]{0:T(128)}, u32[]{:S(2)}) copy-start(f32[128]{0:T(128)} %param.22) | copy-start | bytes 1540
  48.5 18.8 %copy-start.11 = (s32[1,128,4]{1,2,0:T(4,128)S(1)}, s32[1,128,4]{1,2,0:T(4,128)}, u32[]{:S(2)}) copy-start(s32[1,128,4]{1,2,0:T(4,128)} %param.28) | copy-start | bytes 6148
  48.5 18.8 %copy-start.12 = (f32[1,128,4]{1,2,0:T(4,128)S(1)}, f32[1,128,4]{1,2,0:T(4,128)}, u32[]{:S(2)}) copy-start(f32[1,128,4]{1,2,0:T(4,128)} %param.29) | copy-start | bytes 6148
  70.0 4.8 %copy-start.7 = (bf16[1,128,2048]{2,1,0:T(8,128)(2,1)S(1)}, bf16[1,128,2048]{2,1,0:T(8,128)(2,1)}, u32[]{:S(2)}) copy-start(bf16[1,128,2048]{2,1,0:T(8,128)(2,1)} %param.23) | copy-start | bytes 1572868
  70.0 4.8 %copy-start.8 = (f32[2048]{0:T(1024)S(1)}, f32[2048]{0:T(1024)}, u32[]{:S(2)}) copy-start(f32[2048]{0:T(1024)} %param.25) | copy-start | bytes 24580
  74.8 0.7 copy-start.9
  74.8 1.6 copy-start.6
  76.4 3.9 %copy-start.3 = (bf16[128,2048]{1,0:T(8,128)(2,1)}, bf16[128,2048]{1,0:T(8,128)(2,1)S(1)}, u32[]{:S(2)}) copy-start(bf16[128,2048]{1,0:T(8,128)(2,1)S(1)} %fusion.7.normed_ref) | copy-start | bytes 1572868
  190.4 2.1 %copy-start.4 = (bf16[16,24,2048]{2,1,0:T(8,128)(2,1)S(1)}, bf16[16,24,2048]{2,1,0:T(8,128)(2,1)}, u32[]{:S(2)}) copy-start(bf16[16,24,2048]{2,1,0:T(8,128)(2,1)} %get-tuple-element.15) | copy-start | bytes 4718596
  190.4 2.2 %copy-start.5 = (f32[128,2048]{1,0:T(8,128)S(1)}, f32[128,2048]{1,0:T(8,128)}, u32[]{:S(2)}) copy-start(f32[128,2048]{1,0:T(8,128)} %fusion.3) | copy-start | bytes 3145732
  192.5 1.7 copy-start.10
